TPU v7x, 32 devices: a whole 2x2x4 slice. The times are simulated.
32 devices in a mesh: sp: 4 (over y, x), tp: 8 (over z, core).
Axes of the slice: x: 2, y: 2, z: 4, core: 2. Of those that a mesh axis runs over, the one named last changes fastest.
Arguments:
- target: bfloat16 [512, 2048], P('sp'), may hold values from -6 to 6
- source: bfloat16 [1536, 2048], P('sp'), may hold values from -6 to 6
- cotangent: bfloat16 [512, 2048], P('sp'), may hold values from -192 to 192
- target_gain: float32 [2048], replicated, may hold values from 0.1 to 1.9
- source_gain: float32 [2048], replicated, may hold values from 0.1 to 1.9
- w_query: bfloat16 [2048, 4096], P(None, 'tp'), may hold values from -0.125 to 0.125
- w_key: bfloat16 [2048, 128], replicated, may hold values from -0.125 to 0.125
- w_value: bfloat16 [2048, 128], replicated, may hold values from -0.125 to 0.125
- w_out: bfloat16 [4096, 2048], P('tp'), may hold values from -0.09375 to 0.09375
Outputs:
- grad_target: bfloat16 [512, 2048], P(('sp', 'tp'))
- grad_source: bfloat16 [1536, 2048], P(('sp', 'tp'))
- grad_out_w: bfloat16 [4096, 2048], P('tp', 'sp')
All inputs are finite; a program needn't handle non-finite values.
Results may differ from a plain program's by a relative error of at most 0.025.
Values may be sent and summed in bfloat16 or wider, within the bound.
No kernel may reach another device: no remote copies, remote signals or barrier semaphores. Data moves between devices by JAX's collectives and lax.ppermute only.
A program may use at most 64 MiB of HBM per device.

v0:
```python
import functools

import jax
import jax.numpy as jnp
from jax import lax
from jax.experimental import pallas as pl
from jax.experimental.pallas import tpu as pltpu
from jax.sharding import PartitionSpec as P


HEAD = 128
NORM_EPS = 1e-06
LOG2_E = 1.4426950408889634
ROW_TILE = 16

BF16 = jnp.bfloat16
F32 = jnp.float32


VMEM = pl.BlockSpec(memory_space=pltpu.VMEM)
HBM = pl.BlockSpec(memory_space=pltpu.HBM)


def nn(left, right):
    return lax.dot_general(left, right, (((1,), (0,)), ((), ())), preferred_element_type=F32)


def nt(left, right):
    return lax.dot_general(left, right, (((1,), (1,)), ((), ())), preferred_element_type=F32)


def inverse_rms(rows_wide):
    return lax.rsqrt(jnp.mean(rows_wide * rows_wide, axis=1, keepdims=True) + NORM_EPS)


def norm_back(rows, gain, upstream):
    wide = rows.astype(F32)
    inv = inverse_rms(wide)
    unit = wide * inv
    pulled = upstream * gain
    return inv * (pulled - unit * jnp.mean(pulled * unit, axis=1, keepdims=True))


def in_hbm(array):
    return pltpu.with_memory_space_constraint(array, pltpu.HBM)


def shape(dims, kind):
    return jax.ShapeDtypeStruct(dims, kind)


def call(body, outs, flops, moved, in_specs, scratch=()):
    return pl.pallas_call(
        body,
        out_shape=outs,
        in_specs=in_specs,
        out_specs=jax.tree.map(lambda _: VMEM, outs),
        scratch_shapes=scratch,
        cost_estimate=pl.CostEstimate(flops=flops, bytes_accessed=moved, transcendentals=0),
        compiler_params=pltpu.CompilerParams(vmem_limit_bytes=32 * 1024 * 1024),
    )


def block_offsets(blocks):
    half = max(blocks // 2, 1)
    return [2 * (b % half) + b // half for b in range(blocks)]


def order_rows(rows, blocks):
    place = lax.axis_index("tp")
    split = rows.reshape(blocks, rows.shape[0] // blocks, rows.shape[1])
    return jnp.concatenate(
        [lax.dynamic_index_in_dim(split, place ^ off, 0, keepdims=False) for off in block_offsets(blocks)]
    )


def block_copies(source, target, sems, blocks):
    if blocks == 1:
        return [pltpu.make_async_copy(source.at[pl.ds(0, target.shape[0])], target, sems.at[0])]
    rows = source.shape[0] // blocks
    place = lax.axis_index("tp")
    return [
        pltpu.make_async_copy(
            source.at[pl.ds(pl.multiple_of((place ^ off) * rows, ROW_TILE), rows)],
            target.at[pl.ds(b * rows, rows)],
            sems.at[b],
        )
        for b, off in enumerate(block_offsets(blocks)[: target.shape[0] // rows])
    ]


def source_kernel(
    s_blocks, t_blocks, own, sp_count, source, cotangent, gain, w_key, w_value, *rest
):
    messages, rest = rest[:sp_count], rest[sp_count:]
    part, held, held_c, weights, gains, sems, c_sems, w_sems = rest
    copies = block_copies(source, held, sems, s_blocks)
    c_copies = block_copies(cotangent, held_c, c_sems, t_blocks)
    w_copies = [
        pltpu.make_async_copy(w, weights.at[:, pl.ds(n * HEAD, HEAD)], w_sems.at[n])
        for n, w in enumerate((w_key, w_value))
    ]
    w_copies.append(pltpu.make_async_copy(gain, gains, w_sems.at[2]))
    for copy in copies + w_copies + c_copies:
        copy.start()
    for copy in copies + w_copies:
        copy.wait()
    rows, c_rows = held.shape[0], held_c.shape[0]
    wide = held[...].astype(F32)
    acc = nn((wide * gains[...]).astype(BF16), weights[...])
    both = (acc * inverse_rms(wide)).astype(BF16)
    for message in messages:
        message[0:rows, :] = both[:, 0:HEAD]
        message[rows : 2 * rows, :] = both[:, HEAD:]
    part[...] = held[0:own, :]
    for copy in c_copies:
        copy.wait()
    pieces = held_c.shape[1] // (sp_count * HEAD)
    sp_place = lax.axis_index("sp")
    for k, message in enumerate(messages):
        for piece in range(pieces):
            column = pl.multiple_of(((sp_place ^ k) * pieces + piece) * HEAD, HEAD)
            at = 2 * rows + piece * c_rows
            message[at : at + c_rows, :] = held_c[:, pl.ds(column, HEAD)]


def target_kernel(
    blocks, own, target, cotangent, gain, w_query, w_out, q, q_t, da, da_t, part,
    held_t, held_c, gains, weights, sems_t, sems_c, sems,
):
    t_copies = block_copies(target, held_t, sems_t, blocks)
    c_copies = block_copies(cotangent, held_c, sems_c, blocks)
    gain_copy = pltpu.make_async_copy(gain, gains, sems.at[0])
    w_copy = pltpu.make_async_copy(w_out, weights, sems.at[1])
    for copy in t_copies + [gain_copy] + c_copies + [w_copy]:
        copy.start()
    rows = target.shape[0]
    heads = w_out.shape[0] // HEAD
    for copy in t_copies + [gain_copy]:
        copy.wait()
    wide = held_t[...].astype(F32)
    queries = nn((wide * gains[...]).astype(BF16), w_query[...])
    queries = (queries * inverse_rms(wide)).astype(BF16)
    for h in range(heads):
        query = queries[:, h * HEAD : (h + 1) * HEAD]
        q[h * rows : (h + 1) * rows, :] = query
        q_t[:, h * rows : (h + 1) * rows] = query.T
    part[...] = held_t[0:own, :]
    for copy in c_copies + [w_copy]:
        copy.wait()
    grads = nt(held_c[...], weights[...]).astype(BF16)
    for h in range(heads):
        grad = grads[:, h * HEAD : (h + 1) * HEAD]
        da[h * rows : (h + 1) * rows, :] = grad
        da_t[:, h * rows : (h + 1) * rows] = grad.T


def attend_half(half, q_t, da_t, messages, exps, prob_grads, total, out_acc):
    for k, message in enumerate(messages):
        key, value = message[0:half, :], message[half : 2 * half, :]
        exponent = jnp.exp2(nn(key, q_t[...]) * (HEAD ** (-0.5) * LOG2_E))
        total = total + jnp.sum(exponent, axis=0, keepdims=True)
        exps[k * half : (k + 1) * half, :] = exponent
        prob_grads[k * half : (k + 1) * half, :] = nn(value, da_t[...])
        out_acc = out_acc + nn(value.T, exponent.astype(BF16))
    return total, out_acc


def near_kernel(half, sp_count, q_t, da_t, *rest):
    messages, (exps, prob_grads, total, out_acc) = rest[:sp_count], rest[sp_count:]
    total[...], out_acc[...] = attend_half(
        half, q_t, da_t, messages, exps, prob_grads,
        jnp.zeros(total.shape, F32), jnp.zeros(out_acc.shape, F32),
    )


def far_kernel(half, sp_count, q, q_t, da, da_t, near_exps, near_grads, near_total, near_acc, *rest):
    near, far, rest = rest[:sp_count], rest[sp_count : 2 * sp_count], rest[2 * sp_count :]
    att_t, dq, keep, send, far_exps, far_grads = rest
    lanes = q_t.shape[1]
    rows = dq.shape[0]
    heads = lanes // rows
    inv_root = HEAD ** (-0.5)
    total, out_acc = attend_half(
        half, q_t, da_t, far, far_exps, far_grads, near_total[...], near_acc[...]
    )
    inv_total = 1.0 / total
    attended = (out_acc * inv_total).astype(BF16)
    for h in range(heads):
        att_t[h * HEAD : (h + 1) * HEAD, :] = attended[:, h * rows : (h + 1) * rows]
    delta = jnp.sum(attended.astype(F32) * da_t[...].astype(F32), axis=0, keepdims=True)
    dq_acc = jnp.zeros((HEAD, lanes), F32)
    for messages, exps, prob_grads, out in (
        (far, far_exps, far_grads, send),
        (near, near_exps, near_grads, keep),
    ):
        for k in range(sp_count):
            span = slice(k * half, (k + 1) * half)
            probs = exps[span, :] * inv_total
            score_grad = (probs * (prob_grads[span, :] - delta)).astype(BF16)
            at = 2 * k * half
            dkey = nn(score_grad, q[...]) * inv_root
            out[at : at + half, :] = dkey.astype(out.dtype)
            dvalue = nn(probs.astype(BF16), da[...])
            out[at + half : at + 2 * half, :] = dvalue.astype(out.dtype)
            dq_acc = dq_acc + nn(messages[k][0:half, :].T, score_grad)
    dq_t = (dq_acc * inv_root).astype(BF16)
    for h in range(heads):
        dq[:, h * HEAD : (h + 1) * HEAD] = dq_t[:, h * rows : (h + 1) * rows].T


def pull_kernel(dq, w_query, keep, send):
    half = keep.shape[0]
    pulled = nt(dq[...], w_query[...])
    keep[...] = pulled[0:half]
    send[...] = pulled[half:].astype(BF16)


def summed(refs, rows=slice(None)):
    total = refs[0][rows, :].astype(F32)
    for ref in refs[1:]:
        total = total + ref[rows, :].astype(F32)
    return total


def fold_core_kernel(keep, received, *outs):
    step = keep.shape[0] // len(outs)
    for b, out in enumerate(outs):
        out[...] = summed((keep, received), slice(b * step, (b + 1) * step)).astype(BF16)


def fold_sp_kernel(half, count, *refs):
    parts, outs = refs[:count], refs[count:]
    step = half // len(outs)
    for b, out in enumerate(outs):
        for part in range(2):
            at = part * half + b * step
            total = summed(parts, slice(at, at + step))
            out[part * step : (part + 1) * step, :] = total.astype(BF16)


def finish_source_kernel(count, *refs):
    parts, (rows, gain, w_key, w_value, out) = refs[:count], refs[count:]
    grad = summed(parts).astype(BF16)
    own = rows.shape[0]
    pulled = nt(grad[0:own], w_key[...]) + nt(grad[own:], w_value[...])
    out[...] = norm_back(rows[...], gain[...], pulled).astype(BF16)


def finish_target_kernel(count, *refs):
    parts, (rows, gain, out) = refs[:count], refs[count:]
    out[...] = norm_back(rows[...], gain[...], summed(parts)).astype(BF16)


def grad_out_kernel(skip_cot, count, *refs):
    atts, near, far, (out, cots) = (
        refs[:count], refs[count : 2 * count], refs[2 * count : 3 * count], refs[3 * count :]
    )
    pieces = out.shape[1] // HEAD
    rows = cots.shape[0] // 2
    total = jnp.zeros(out.shape, F32)
    for att, pair in zip(atts, zip(near, far)):
        for side, message in enumerate(pair):
            for piece in range(pieces):
                at = skip_cot + piece * rows
                cots[side * rows : (side + 1) * rows, piece * HEAD : (piece + 1) * HEAD] = message[
                    at : at + rows, :
                ]
        total = total + nn(att[...], cots[...])
    out[...] = total.astype(BF16)


def on_device(target, source, cotangent, target_gain, source_gain, w_query, w_key, w_value, w_out):
    tp_count, sp_count = lax.axis_size("tp"), lax.axis_size("sp")
    z_count = tp_count // 2
    t_rows, s_rows = target.shape[0], source.shape[0]
    width = target.shape[1]
    t_own, s_own = t_rows // tp_count, s_rows // tp_count
    q_width = w_query.shape[1]
    heads = q_width // HEAD
    lanes = heads * t_rows
    target_gain, source_gain = target_gain[None, :], source_gain[None, :]

    def swap(value, axis, count, offset):
        return lax.ppermute(value, axis, [(i, i ^ offset) for i in range(count)])

    def to_sp(values):
        return [values[0]] + [swap(values[k], "sp", sp_count, k) for k in range(1, sp_count)]

    def to_z(values):
        return [values[0]] + [swap(values[k], "tp", tp_count, 2 * k) for k in range(1, z_count)]

    def to_core(value):
        return swap(value, "tp", tp_count, 1)

    s_blocks = tp_count if s_own % ROW_TILE == 0 else 1
    t_blocks = tp_count if t_own % ROW_TILE == 0 else 1
    if s_blocks == 1:
        source = order_rows(source, tp_count)
    if t_blocks == 1:
        target, cotangent = order_rows(target, tp_count), order_rows(cotangent, tp_count)
    s_half, t_half = s_rows // 2, t_rows // 2
    far_rows = sp_count * s_half
    cot_rows = width // sp_count // HEAD * t_half

    *near, source_part = call(
        functools.partial(source_kernel, s_blocks, t_blocks, s_own, sp_count),
        [shape((2 * s_half + cot_rows, HEAD), BF16)] * sp_count + [shape((s_own, width), BF16)],
        4 * s_half * width * HEAD, s_rows * width * 2 + 4 * width * HEAD,
        [HBM] * 5,
        [
            pltpu.VMEM((s_half, width), BF16),
            pltpu.VMEM((t_half, width), BF16),
            pltpu.VMEM((width, 2 * HEAD), BF16),
            pltpu.VMEM((1, width), F32),
        ]
        + [pltpu.SemaphoreType.DMA((n,)) for n in (s_blocks, t_blocks, 3)],
    )(*map(in_hbm, (source, cotangent, source_gain, w_key, w_value)))
    near = to_sp(near)
    far = [to_core(message) for message in near]

    q, q_t, da, da_t, target_part = call(
        functools.partial(target_kernel, t_blocks, t_own),
        [shape((lanes, HEAD), BF16), shape((HEAD, lanes), BF16)] * 2
        + [shape((t_own, width), BF16)],
        4 * t_rows * width * q_width, 4 * width * q_width + 4 * t_rows * width,
        [HBM, HBM, HBM, VMEM, HBM],
        [pltpu.VMEM((t_rows, width), BF16)] * 2
        + [pltpu.VMEM((1, width), F32), pltpu.VMEM((q_width, width), BF16)]
        + [pltpu.SemaphoreType.DMA((n,)) for n in (t_blocks, t_blocks, 2)],
    )(in_hbm(target), in_hbm(cotangent), in_hbm(target_gain), w_query, in_hbm(w_out))

    stats = call(
        functools.partial(near_kernel, s_half, sp_count),
        [shape((far_rows, lanes), F32)] * 2 + [shape((1, lanes), F32), shape((HEAD, lanes), F32)],
        6 * lanes * far_rows * HEAD, 8 * far_rows * lanes,
        [VMEM] * (2 + sp_count), (),
    )(q_t, da_t, *near)
    att_t, dq, keep, send = call(
        functools.partial(far_kernel, s_half, sp_count),
        [
            shape((q_width, t_rows), BF16),
            shape((t_rows, q_width), BF16),
            shape((2 * far_rows, HEAD), F32),
            shape((2 * far_rows, HEAD), BF16),
        ],
        18 * lanes * far_rows * HEAD, 8 * far_rows * lanes,
        [VMEM] * (8 + 2 * sp_count), [pltpu.VMEM((far_rows, lanes), F32)] * 2,
    )(q, q_t, da, da_t, *stats, *near, *far)

    received = to_core(send)
    t_keep, t_send = call(
        pull_kernel,
        [shape((t_half, width), F32), shape((t_half, width), BF16)],
        2 * t_rows * width * q_width, 2 * width * q_width + 8 * t_rows * width,
        [VMEM, VMEM], (),
    )(dq, w_query)
    t_received = to_core(t_send)
    grads = call(
        fold_core_kernel, [shape((2 * s_half, HEAD), BF16)] * sp_count,
        2 * far_rows * HEAD, 16 * far_rows * HEAD, [VMEM] * 2, (),
    )(keep, received)
    atts = to_sp([att_t] * sp_count)
    grads = to_sp(grads)

    pieces = z_count if t_blocks > 1 else 1
    t_parts = call(
        fold_core_kernel, [shape((t_half // pieces, width), BF16)] * pieces,
        t_half * width, 8 * t_half * width, [VMEM] * 2, (),
    )(t_keep, t_received)
    if t_blocks == 1:
        t_parts = [t_parts[0][b * t_own : (b + 1) * t_own] for b in range(z_count)]
    t_parts = to_z(t_parts)

    pieces = z_count if s_blocks > 1 else 1
    s_parts = call(
        functools.partial(fold_sp_kernel, s_half, sp_count),
        [shape((2 * s_half // pieces, HEAD), BF16)] * pieces,
        2 * s_half * HEAD * sp_count, 16 * s_half * HEAD, [VMEM] * sp_count, (),
    )(*grads)
    if s_blocks == 1:
        both = s_parts[0].reshape(2, z_count, s_own, HEAD)
        s_parts = [both[:, b].reshape(2 * s_own, HEAD) for b in range(z_count)]
    s_parts = to_z(s_parts)

    grad_target = call(
        functools.partial(finish_target_kernel, z_count), shape((t_own, width), BF16),
        10 * t_own * width, 8 * t_own * width, [VMEM] * (z_count + 2), (),
    )(*t_parts, target_part, target_gain)
    grad_out = call(
        functools.partial(grad_out_kernel, 2 * s_half, sp_count),
        shape((q_width, width // sp_count), BF16),
        2 * q_width * width * t_rows, 2 * q_width * width, [VMEM] * (3 * sp_count),
        [pltpu.VMEM((t_rows, width // sp_count), BF16)],
    )(*atts, *near, *far)
    grad_source = call(
        functools.partial(finish_source_kernel, z_count), shape((s_own, width), BF16),
        4 * s_own * width * HEAD, 4 * width * HEAD, [VMEM] * (z_count + 4), (),
    )(*s_parts, source_part, source_gain, w_key, w_value)
    return (grad_target, grad_source, grad_out)


def solution(mesh):
    in_specs = (
        P("sp", None),
        P("sp", None),
        P("sp", None),
        P(),
        P(),
        P(None, "tp"),
        P(),
        P(),
        P("tp", None),
    )
    out_specs = (P(("sp", "tp"), None), P(("sp", "tp"), None), P("tp", "sp"))

    return jax.shard_map(
        on_device, mesh=mesh, in_specs=in_specs, out_specs=out_specs, check_vma=False
    )
```

profile of v0, /device:TPU:0, one launch (start us, length us, event | category | flops | bytes accessed | tf_op | source)
XLA Modules:
  0.0 49.1 jit_solution(7581786746339912393)
XLA Ops:
  0.6 2.3 %shard_map.113 = (bf16[640,128]{1,0:T(8,128)(2,1)S(1)}, bf16[640,128]{1,0:T(8,128)(2,1)S(1)}, bf16[640,128]{1,0:T(8,128)(2,1)S(1)}, bf16[640,128]{1,0:T(8,128)(2,1)S(1)}, bf16[48,2048]{1,0:T(8,128)(2,1)S(1)}) custom-call(bf16[384,2048]{1,0:T(8,128)(2,1)} %source.1, bf16[128,2048]{1,0:T(8,128)(2,1)} %cotangent.3, f32[1,2048]{1,0:T(1,128)} %bitcast.2, ...), custom_call_target="tpu_custom_call" | custom-call | flops 201326592 | bytes 2621440 | tf_op jit(solution)/shard_map/pallas_call | solution.py:306
  3.0 3.0 %collective-permute-start = (bf16[640,128]{1,0:T(8,128)(2,1)S(1)}, bf16[640,128]{1,0:T(8,128)(2,1)S(1)}, u32[]{:S(2)}, u32[]{:S(2)}) collective-permute-start(bf16[640,128]{1,0:T(8,128)(2,1)S(1)} %get-tuple-element.40), channel_id=1, source_target_pairs={{0,8},{8,0},{16,24},{24,16},{1,9},{9,1},{17,25},{25,17},{2,10},{10... | collective-permute-start | bytes 491528 | tf_op jit(solution)/shard_map/ppermute | solution.py:285
  6.0 1.5 %collective-permute-start.1 = (bf16[640,128]{1,0:T(8,128)(2,1)S(1)}, bf16[640,128]{1,0:T(8,128)(2,1)S(1)}, u32[]{:S(2)}, u32[]{:S(2)}) collective-permute-start(bf16[640,128]{1,0:T(8,128)(2,1)S(1)} %get-tuple-element.41), channel_id=1, source_target_pairs={{0,16},{8,24},{16,0},{24,8},{1,17},{9,25},{17,1},{25,9},{2,18},{10... | collective-permute-start | bytes 491528 | tf_op jit(solution)/shard_map/ppermute | solution.py:285
  7.5 0.0 collective-permute-start.2
  7.5 0.0 collective-permute-start.3
  7.5 3.5 %collective-permute-done.rest_1_.refs_5_ = bf16[640,128]{1,0:T(8,128)(2,1)S(1)} collective-permute-done((bf16[640,128]{1,0:T(8,128)(2,1)S(1)}, bf16[640,128]{1,0:T(8,128)(2,1)S(1)}, u32[]{:S(2)}, u32[]{:S(2)}) %collective-permute-start) | collective-permute-done | bytes 163872 | tf_op jit(solution)/shard_map/ppermute | solution.py:285
  11.0 0.0 collective-permute-start.4
  11.0 4.1 %collective-permute-done.1.rest_2_.refs_6_ = bf16[640,128]{1,0:T(8,128)(2,1)S(1)} collective-permute-done((bf16[640,128]{1,0:T(8,128)(2,1)S(1)}, bf16[640,128]{1,0:T(8,128)(2,1)S(1)}, u32[]{:S(2)}, u32[]{:S(2)}) %collective-permute-start.1) | collective-permute-done | bytes 163872 | tf_op jit(solution)/shard_map/ppermute | solution.py:285
  15.2 0.0 collective-permute-start.5
  15.2 0.0 collective-permute-done.2.rest_3_.refs_7_
  15.2 0.5 %collective-permute-start.6 = (bf16[640,128]{1,0:T(8,128)(2,1)S(1)}, bf16[640,128]{1,0:T(8,128)(2,1)S(1)}, u32[]{:S(2)}, u32[]{:S(2)}) collective-permute-start(bf16[640,128]{1,0:T(8,128)(2,1)S(1)} %collective-permute-done.2.rest_3_.refs_7_), channel_id=1, source_target_pairs={{0,1},{1,0},{2,3},{3,2},{4,5},{5,4},{6,7},{7,6},{8,9},{9,8},{10,11... | collective-permute-start | bytes 491528 | tf_op jit(solution)/shard_map/ppermute | solution.py:285
  15.7 3.1 %shard_map.112 = (bf16[512,128]{1,0:T(8,128)(2,1)S(1)}, bf16[128,512]{1,0:T(8,128)(2,1)S(1)}, bf16[512,128]{1,0:T(8,128)(2,1)S(1)}, bf16[128,512]{1,0:T(8,128)(2,1)S(1)}, bf16[16,2048]{1,0:T(8,128)(2,1)S(1)}) custom-call(bf16[128,2048]{1,0:T(8,128)(2,1)} %target.1, bf16[128,2048]{1,0:T(8,128)(2,1)} %cotangent.3, f32[1,2048]{1,0:T(1,128)} %bitcast.4, ...), custom_call_target="tpu_custom_call" | custom-call | flops 536870912 | bytes 5242880 | tf_op jit(solution)/shard_map/pallas_call | solution.py:322
  18.8 1.0 %shard_map.114 = (f32[768,512]{1,0:T(8,128)S(1)}, f32[768,512]{1,0:T(8,128)S(1)}, f32[1,512]{1,0:T(1,128)S(1)}, f32[128,512]{1,0:T(8,128)S(1)}) custom-call(bf16[128,512]{1,0:T(8,128)(2,1)S(1)} %get-tuple-element.36.q_t, bf16[128,512]{1,0:T(8,128)(2,1)S(1)} %get-tuple-element.38.da_t, bf16[640,128]{1,0:T(8,128)(2,1)S(1)} %get-tuple-element.39.rest_0_.refs_4_, ...), custom_call_target="tpu_custom_call" | custom-call | flops 301989888 | bytes 3145728 | tf_op jit(solution)/shard_map/pallas_call | solution.py:333
  19.8 0.0 collective-permute-done.3.rest_4_.refs_8_
  19.8 0.0 collective-permute-done.4.rest_5_.refs_9_
  19.8 0.0 collective-permute-done.5.rest_6_.refs_10_
  19.8 0.0 collective-permute-done.6.rest_7_.refs_11_
  19.8 2.7 %shard_map.115 = (bf16[512,128]{1,0:T(8,128)(2,1)S(1)}, bf16[128,512]{1,0:T(8,128)(2,1)S(1)}, f32[1536,128]{1,0:T(8,128)S(1)}, bf16[1536,128]{1,0:T(8,128)(2,1)S(1)}) custom-call(bf16[512,128]{1,0:T(8,128)(2,1)S(1)} %get-tuple-element.35.q, bf16[128,512]{1,0:T(8,128)(2,1)S(1)} %get-tuple-element.36.q_t, bf16[512,128]{1,0:T(8,128)(2,1)S(1)} %get-tuple-element.37.da, ...), custom_call_target="tpu_custom_call" | custom-call | flops 905969664 | bytes 3145728 | tf_op jit(solution)/shard_map/pallas_call | solution.py:339
  22.5 0.1 collective-permute-start.11
  22.6 0.8 %shard_map.116 = (f32[64,2048]{1,0:T(8,128)S(1)}, bf16[64,2048]{1,0:T(8,128)(2,1)S(1)}) custom-call(bf16[128,512]{1,0:T(8,128)(2,1)S(1)} %get-tuple-element.47.dq, bf16[2048,512]{1,0:T(8,128)(2,1)S(1)} %copy-done), custom_call_target="tpu_custom_call" | custom-call | flops 268435456 | bytes 4194304 | tf_op jit(solution)/shard_map/pallas_call | solution.py:352
  23.4 0.6 %collective-permute-start.7 = (bf16[64,2048]{1,0:T(8,128)(2,1)S(1)}, bf16[64,2048]{1,0:T(8,128)(2,1)S(1)}, u32[]{:S(2)}, u32[]{:S(2)}) collective-permute-start(bf16[64,2048]{1,0:T(8,128)(2,1)S(1)} %get-tuple-element.49), channel_id=1, source_target_pairs={{0,1},{1,0},{2,3},{3,2},{4,5},{5,4},{6,7},{7,6},{8,9},{9,8},{10,11... | collective-permute-start | bytes 786440 | tf_op jit(solution)/shard_map/ppermute | solution.py:285
  24.0 1.5 %collective-permute-start.20 = (bf16[512,128]{1,0:T(8,128)(2,1)S(1)}, bf16[512,128]{1,0:T(8,128)(2,1)S(1)}, u32[]{:S(2)}, u32[]{:S(2)}) collective-permute-start(bf16[512,128]{1,0:T(8,128)(2,1)S(1)} %get-tuple-element.66.refs_0_), channel_id=1, source_target_pairs={{0,24},{8,16},{16,8},{24,0},{1,25},{9,17},{17,9},{25,1},{2,26},{10... | collective-permute-start | bytes 393224 | tf_op jit(solution)/shard_map/ppermute | solution.py:285
  25.5 0.0 collective-permute-done.11.received
  25.5 0.1 shard_map.119
  25.5 1.6 %collective-permute-start.12 = (bf16[384,128]{1,0:T(8,128)(2,1)S(1)}, bf16[384,128]{1,0:T(8,128)(2,1)S(1)}, u32[]{:S(2)}, u32[]{:S(2)}) collective-permute-start(bf16[384,128]{1,0:T(8,128)(2,1)S(1)} %get-tuple-element.58), channel_id=1, source_target_pairs={{0,8},{8,0},{16,24},{24,16},{1,9},{9,1},{17,25},{25,17},{2,10},{10... | collective-permute-start | bytes 294920 | tf_op jit(solution)/shard_map/ppermute | solution.py:285
  27.1 0.5 %collective-permute-start.13 = (bf16[384,128]{1,0:T(8,128)(2,1)S(1)}, bf16[384,128]{1,0:T(8,128)(2,1)S(1)}, u32[]{:S(2)}, u32[]{:S(2)}) collective-permute-start(bf16[384,128]{1,0:T(8,128)(2,1)S(1)} %get-tuple-element.59), channel_id=1, source_target_pairs={{0,16},{8,24},{16,0},{24,8},{1,17},{9,25},{17,1},{25,9},{2,18},{10... | collective-permute-start | bytes 294920 | tf_op jit(solution)/shard_map/ppermute | solution.py:285
  27.6 1.5 %collective-permute-start.14 = (bf16[384,128]{1,0:T(8,128)(2,1)S(1)}, bf16[384,128]{1,0:T(8,128)(2,1)S(1)}, u32[]{:S(2)}, u32[]{:S(2)}) collective-permute-start(bf16[384,128]{1,0:T(8,128)(2,1)S(1)} %get-tuple-element.60), channel_id=1, source_target_pairs={{0,24},{8,16},{16,8},{24,0},{1,25},{9,17},{17,9},{25,1},{2,26},{10... | collective-permute-start | bytes 294920 | tf_op jit(solution)/shard_map/ppermute | solution.py:285
  29.1 2.1 %collective-permute-done.20.refs_3_ = bf16[512,128]{1,0:T(8,128)(2,1)S(1)} collective-permute-done((bf16[512,128]{1,0:T(8,128)(2,1)S(1)}, bf16[512,128]{1,0:T(8,128)(2,1)S(1)}, u32[]{:S(2)}, u32[]{:S(2)}) %collective-permute-start.20) | collective-permute-done | bytes 131104 | tf_op jit(solution)/shard_map/ppermute | solution.py:285
  31.2 1.5 %collective-permute-start.19 = (bf16[512,128]{1,0:T(8,128)(2,1)S(1)}, bf16[512,128]{1,0:T(8,128)(2,1)S(1)}, u32[]{:S(2)}, u32[]{:S(2)}) collective-permute-start(bf16[512,128]{1,0:T(8,128)(2,1)S(1)} %get-tuple-element.66.refs_0_), channel_id=1, source_target_pairs={{0,16},{8,24},{16,0},{24,8},{1,17},{9,25},{17,1},{25,9},{2,18},{10... | collective-permute-start | bytes 393224 | tf_op jit(solution)/shard_map/ppermute | solution.py:285
  32.8 0.0 collective-permute-done.7.received
  32.8 0.5 %collective-permute-start.18 = (bf16[512,128]{1,0:T(8,128)(2,1)S(1)}, bf16[512,128]{1,0:T(8,128)(2,1)S(1)}, u32[]{:S(2)}, u32[]{:S(2)}) collective-permute-start(bf16[512,128]{1,0:T(8,128)(2,1)S(1)} %get-tuple-element.66.refs_0_), channel_id=1, source_target_pairs={{0,8},{8,0},{16,24},{24,16},{1,9},{9,1},{17,25},{25,17},{2,10},{10... | collective-permute-start | bytes 393224 | tf_op jit(solution)/shard_map/ppermute | solution.py:285
  33.3 0.1 shard_map.117
  33.4 0.0 copy-start.4
  33.4 0.0 collective-permute-done.12.refs_1_
  33.4 1.6 %collective-permute-start.8 = (bf16[16,2048]{1,0:T(8,128)(2,1)S(1)}, bf16[16,2048]{1,0:T(8,128)(2,1)S(1)}, u32[]{:S(2)}, u32[]{:S(2)}) collective-permute-start(bf16[16,2048]{1,0:T(8,128)(2,1)S(1)} %get-tuple-element.51), channel_id=1, source_target_pairs={{0,2},{1,3},{2,0},{3,1},{4,6},{5,7},{6,4},{7,5},{8,10},{9,11},{10,... | collective-permute-start | bytes 196616 | tf_op jit(solution)/shard_map/ppermute | solution.py:285
  35.0 2.6 %collective-permute-start.9 = (bf16[16,2048]{1,0:T(8,128)(2,1)S(1)}, bf16[16,2048]{1,0:T(8,128)(2,1)S(1)}, u32[]{:S(2)}, u32[]{:S(2)}) collective-permute-start(bf16[16,2048]{1,0:T(8,128)(2,1)S(1)} %get-tuple-element.52), channel_id=1, source_target_pairs={{0,4},{1,5},{2,6},{3,7},{4,0},{5,1},{6,2},{7,3},{8,12},{9,13},{10,... | collective-permute-start | bytes 196616 | tf_op jit(solution)/shard_map/ppermute | solution.py:285
  37.6 0.0 collective-permute-done.14.refs_3_
  37.6 1.4 %collective-permute-start.10 = (bf16[16,2048]{1,0:T(8,128)(2,1)S(1)}, bf16[16,2048]{1,0:T(8,128)(2,1)S(1)}, u32[]{:S(2)}, u32[]{:S(2)}) collective-permute-start(bf16[16,2048]{1,0:T(8,128)(2,1)S(1)} %get-tuple-element.53), channel_id=1, source_target_pairs={{0,6},{1,7},{2,4},{3,5},{4,2},{5,3},{6,0},{7,1},{8,14},{9,15},{10,... | collective-permute-start | bytes 196616 | tf_op jit(solution)/shard_map/ppermute | solution.py:285
  39.1 0.1 shard_map.120
  39.1 0.1 collective-permute-start.15
  39.2 2.9 %collective-permute-start.16 = (bf16[96,128]{1,0:T(8,128)(2,1)S(1)}, bf16[96,128]{1,0:T(8,128)(2,1)S(1)}, u32[]{:S(2)}, u32[]{:S(2)}) collective-permute-start(bf16[96,128]{1,0:T(8,128)(2,1)S(1)} %get-tuple-element.63), channel_id=1, source_target_pairs={{0,4},{1,5},{2,6},{3,7},{4,0},{5,1},{6,2},{7,3},{8,12},{9,13},{10,... | collective-permute-start | bytes 73736 | tf_op jit(solution)/shard_map/ppermute | solution.py:285
  42.2 1.4 %collective-permute-start.17 = (bf16[96,128]{1,0:T(8,128)(2,1)S(1)}, bf16[96,128]{1,0:T(8,128)(2,1)S(1)}, u32[]{:S(2)}, u32[]{:S(2)}) collective-permute-start(bf16[96,128]{1,0:T(8,128)(2,1)S(1)} %get-tuple-element.64), channel_id=1, source_target_pairs={{0,6},{1,7},{2,4},{3,5},{4,2},{5,3},{6,0},{7,1},{8,14},{9,15},{10,... | collective-permute-start | bytes 73736 | tf_op jit(solution)/shard_map/ppermute | solution.py:285
  43.6 1.6 %shard_map.122 = bf16[512,512]{1,0:T(8,128)(2,1)} custom-call(bf16[512,128]{1,0:T(8,128)(2,1)S(1)} %get-tuple-element.66.refs_0_, bf16[512,128]{1,0:T(8,128)(2,1)S(1)} %collective-permute-done.18.refs_1_, bf16[512,128]{1,0:T(8,128)(2,1)S(1)} %collective-permute-done.19.refs_2_, bf16[512,128]{1,0:T(8,128)(2,1)S(1)} %collective-permute-done.20.refs_3_, ...), custom_call_target="tpu_custom_call" | custom-call | flops 268435456 | bytes 2097152 | tf_op jit(solution)/shard_map/pallas_call | solution.py:390
  45.2 0.8 %shard_map.118 = bf16[16,2048]{1,0:T(8,128)(2,1)} custom-call(bf16[16,2048]{1,0:T(8,128)(2,1)S(1)} %get-tuple-element.50.refs_0_, bf16[16,2048]{1,0:T(8,128)(2,1)S(1)} %collective-permute-done.8.refs_1_, bf16[16,2048]{1,0:T(8,128)(2,1)S(1)} %collective-permute-done.9.refs_2_, bf16[16,2048]{1,0:T(8,128)(2,1)S(1)} %collective-permute-done.10.refs_3_, ...), custom_call_target="tpu_custom_call" | custom-call | flops 327680 | bytes 262144 | tf_op jit(solution)/shard_map/pallas_call | solution.py:386
  46.0 0.0 collective-permute-done.15.refs_1_
  46.0 0.0 collective-permute-done.16.refs_2_
  46.0 1.8 %collective-permute-done.17.refs_3_ = bf16[96,128]{1,0:T(8,128)(2,1)S(1)} collective-permute-done((bf16[96,128]{1,0:T(8,128)(2,1)S(1)}, bf16[96,128]{1,0:T(8,128)(2,1)S(1)}, u32[]{:S(2)}, u32[]{:S(2)}) %collective-permute-start.17) | collective-permute-done | bytes 24608 | tf_op jit(solution)/shard_map/ppermute | solution.py:285
  47.8 1.3 %shard_map.121 = bf16[48,2048]{1,0:T(8,128)(2,1)} custom-call(bf16[96,128]{1,0:T(8,128)(2,1)S(1)} %get-tuple-element.61.refs_0_, bf16[96,128]{1,0:T(8,128)(2,1)S(1)} %collective-permute-done.15.refs_1_, bf16[96,128]{1,0:T(8,128)(2,1)S(1)} %collective-permute-done.16.refs_2_, bf16[96,128]{1,0:T(8,128)(2,1)S(1)} %collective-permute-done.17.refs_3_, ...), custom_call_target="tpu_custom_call" | custom-call | flops 50331648 | bytes 1048576 | tf_op jit(solution)/shard_map/pallas_call | solution.py:396
  (15 shorter events, 0.0 us)
Async XLA Ops:
  0.6 15.0 %copy-start = (bf16[2048,512]{1,0:T(8,128)(2,1)S(1)}, bf16[2048,512]{1,0:T(8,128)(2,1)}, u32[]{:S(2)}) copy-start(bf16[2048,512]{1,0:T(8,128)(2,1)} %w_query.3) | copy-start | bytes 6291460
  3.0 8.1 %collective-permute-start = (bf16[640,128]{1,0:T(8,128)(2,1)S(1)}, bf16[640,128]{1,0:T(8,128)(2,1)S(1)}, u32[]{:S(2)}, u32[]{:S(2)}) collective-permute-start(bf16[640,128]{1,0:T(8,128)(2,1)S(1)} %get-tuple-element.40), channel_id=1, source_target_pairs={{0,8},{8,0},{16,24},{24,16},{1,9},{9,1},{17,25},{25,17},{2,10},{10... | collective-permute-start | bytes 491528 | tf_op jit(solution)/shard_map/ppermute | solution.py:285
  6.0 9.2 %collective-permute-start.1 = (bf16[640,128]{1,0:T(8,128)(2,1)S(1)}, bf16[640,128]{1,0:T(8,128)(2,1)S(1)}, u32[]{:S(2)}, u32[]{:S(2)}) collective-permute-start(bf16[640,128]{1,0:T(8,128)(2,1)S(1)} %get-tuple-element.41), channel_id=1, source_target_pairs={{0,16},{8,24},{16,0},{24,8},{1,17},{9,25},{17,1},{25,9},{2,18},{10... | collective-permute-start | bytes 491528 | tf_op jit(solution)/shard_map/ppermute | solution.py:285
  7.5 7.7 %collective-permute-start.2 = (bf16[640,128]{1,0:T(8,128)(2,1)S(1)}, bf16[640,128]{1,0:T(8,128)(2,1)S(1)}, u32[]{:S(2)}, u32[]{:S(2)}) collective-permute-start(bf16[640,128]{1,0:T(8,128)(2,1)S(1)} %get-tuple-element.42), channel_id=1, source_target_pairs={{0,24},{8,16},{16,8},{24,0},{1,25},{9,17},{17,9},{25,1},{2,26},{10... | collective-permute-start | bytes 491528 | tf_op jit(solution)/shard_map/ppermute | solution.py:285
  7.5 12.2 %collective-permute-start.3 = (bf16[640,128]{1,0:T(8,128)(2,1)S(1)}, bf16[640,128]{1,0:T(8,128)(2,1)S(1)}, u32[]{:S(2)}, u32[]{:S(2)}) collective-permute-start(bf16[640,128]{1,0:T(8,128)(2,1)S(1)} %get-tuple-element.39.rest_0_.refs_4_), channel_id=1, source_target_pairs={{0,1},{1,0},{2,3},{3,2},{4,5},{5,4},{6,7},{7,6},{8,9},{9,8},{10,11... | collective-permute-start | bytes 491528 | tf_op jit(solution)/shard_map/ppermute | solution.py:285
  11.0 8.7 %collective-permute-start.4 = (bf16[640,128]{1,0:T(8,128)(2,1)S(1)}, bf16[640,128]{1,0:T(8,128)(2,1)S(1)}, u32[]{:S(2)}, u32[]{:S(2)}) collective-permute-start(bf16[640,128]{1,0:T(8,128)(2,1)S(1)} %collective-permute-done.rest_1_.refs_5_), channel_id=1, source_target_pairs={{0,1},{1,0},{2,3},{3,2},{4,5},{5,4},{6,7},{7,6},{8,9},{9,8},{10,11... | collective-permute-start | bytes 491528 | tf_op jit(solution)/shard_map/ppermute | solution.py:285
  15.2 4.6 %collective-permute-start.5 = (bf16[640,128]{1,0:T(8,128)(2,1)S(1)}, bf16[640,128]{1,0:T(8,128)(2,1)S(1)}, u32[]{:S(2)}, u32[]{:S(2)}) collective-permute-start(bf16[640,128]{1,0:T(8,128)(2,1)S(1)} %collective-permute-done.1.rest_2_.refs_6_), channel_id=1, source_target_pairs={{0,1},{1,0},{2,3},{3,2},{4,5},{5,4},{6,7},{7,6},{8,9},{9,8},{10,11... | collective-permute-start | bytes 491528 | tf_op jit(solution)/shard_map/ppermute | solution.py:285
  15.2 4.6 %collective-permute-start.6 = (bf16[640,128]{1,0:T(8,128)(2,1)S(1)}, bf16[640,128]{1,0:T(8,128)(2,1)S(1)}, u32[]{:S(2)}, u32[]{:S(2)}) collective-permute-start(bf16[640,128]{1,0:T(8,128)(2,1)S(1)} %collective-permute-done.2.rest_3_.refs_7_), channel_id=1, source_target_pairs={{0,1},{1,0},{2,3},{3,2},{4,5},{5,4},{6,7},{7,6},{8,9},{9,8},{10,11... | collective-permute-start | bytes 491528 | tf_op jit(solution)/shard_map/ppermute | solution.py:285
  22.5 3.0 %collective-permute-start.11 = (bf16[1536,128]{1,0:T(8,128)(2,1)S(1)}, bf16[1536,128]{1,0:T(8,128)(2,1)S(1)}, u32[]{:S(2)}, u32[]{:S(2)}) collective-permute-start(bf16[1536,128]{1,0:T(8,128)(2,1)S(1)} %get-tuple-element.56), channel_id=1, source_target_pairs={{0,1},{1,0},{2,3},{3,2},{4,5},{5,4},{6,7},{7,6},{8,9},{9,8},{10,11... | collective-permute-start | bytes 1179656 | tf_op jit(solution)/shard_map/ppermute | solution.py:285
  23.4 9.4 %collective-permute-start.7 = (bf16[64,2048]{1,0:T(8,128)(2,1)S(1)}, bf16[64,2048]{1,0:T(8,128)(2,1)S(1)}, u32[]{:S(2)}, u32[]{:S(2)}) collective-permute-start(bf16[64,2048]{1,0:T(8,128)(2,1)S(1)} %get-tuple-element.49), channel_id=1, source_target_pairs={{0,1},{1,0},{2,3},{3,2},{4,5},{5,4},{6,7},{7,6},{8,9},{9,8},{10,11... | collective-permute-start | bytes 786440 | tf_op jit(solution)/shard_map/ppermute | solution.py:285
  24.0 7.3 %collective-permute-start.20 = (bf16[512,128]{1,0:T(8,128)(2,1)S(1)}, bf16[512,128]{1,0:T(8,128)(2,1)S(1)}, u32[]{:S(2)}, u32[]{:S(2)}) collective-permute-start(bf16[512,128]{1,0:T(8,128)(2,1)S(1)} %get-tuple-element.66.refs_0_), channel_id=1, source_target_pairs={{0,24},{8,16},{16,8},{24,0},{1,25},{9,17},{17,9},{25,1},{2,26},{10... | collective-permute-start | bytes 393224 | tf_op jit(solution)/shard_map/ppermute | solution.py:285
  25.5 7.9 %collective-permute-start.12 = (bf16[384,128]{1,0:T(8,128)(2,1)S(1)}, bf16[384,128]{1,0:T(8,128)(2,1)S(1)}, u32[]{:S(2)}, u32[]{:S(2)}) collective-permute-start(bf16[384,128]{1,0:T(8,128)(2,1)S(1)} %get-tuple-element.58), channel_id=1, source_target_pairs={{0,8},{8,0},{16,24},{24,16},{1,9},{9,1},{17,25},{25,17},{2,10},{10... | collective-permute-start | bytes 294920 | tf_op jit(solution)/shard_map/ppermute | solution.py:285
  27.1 7.9 %collective-permute-start.13 = (bf16[384,128]{1,0:T(8,128)(2,1)S(1)}, bf16[384,128]{1,0:T(8,128)(2,1)S(1)}, u32[]{:S(2)}, u32[]{:S(2)}) collective-permute-start(bf16[384,128]{1,0:T(8,128)(2,1)S(1)} %get-tuple-element.59), channel_id=1, source_target_pairs={{0,16},{8,24},{16,0},{24,8},{1,17},{9,25},{17,1},{25,9},{2,18},{10... | collective-permute-start | bytes 294920 | tf_op jit(solution)/shard_map/ppermute | solution.py:285
  27.6 10.0 %collective-permute-start.14 = (bf16[384,128]{1,0:T(8,128)(2,1)S(1)}, bf16[384,128]{1,0:T(8,128)(2,1)S(1)}, u32[]{:S(2)}, u32[]{:S(2)}) collective-permute-start(bf16[384,128]{1,0:T(8,128)(2,1)S(1)} %get-tuple-element.60), channel_id=1, source_target_pairs={{0,24},{8,16},{16,8},{24,0},{1,25},{9,17},{17,9},{25,1},{2,26},{10... | collective-permute-start | bytes 294920 | tf_op jit(solution)/shard_map/ppermute | solution.py:285
  31.2 7.9 %collective-permute-start.19 = (bf16[512,128]{1,0:T(8,128)(2,1)S(1)}, bf16[512,128]{1,0:T(8,128)(2,1)S(1)}, u32[]{:S(2)}, u32[]{:S(2)}) collective-permute-start(bf16[512,128]{1,0:T(8,128)(2,1)S(1)} %get-tuple-element.66.refs_0_), channel_id=1, source_target_pairs={{0,16},{8,24},{16,0},{24,8},{1,17},{9,25},{17,1},{25,9},{2,18},{10... | collective-permute-start | bytes 393224 | tf_op jit(solution)/shard_map/ppermute | solution.py:285
  32.8 6.4 %collective-permute-start.18 = (bf16[512,128]{1,0:T(8,128)(2,1)S(1)}, bf16[512,128]{1,0:T(8,128)(2,1)S(1)}, u32[]{:S(2)}, u32[]{:S(2)}) collective-permute-start(bf16[512,128]{1,0:T(8,128)(2,1)S(1)} %get-tuple-element.66.refs_0_), channel_id=1, source_target_pairs={{0,8},{8,0},{16,24},{24,16},{1,9},{9,1},{17,25},{25,17},{2,10},{10... | collective-permute-start | bytes 393224 | tf_op jit(solution)/shard_map/ppermute | solution.py:285
  33.4 11.8 %copy-start.4 = (f32[2048]{0:T(1024)S(1)}, f32[2048]{0:T(1024)}, u32[]{:S(2)}) copy-start(f32[2048]{0:T(1024)} %param.12) | copy-start | bytes 24580
  33.4 8.8 %collective-permute-start.8 = (bf16[16,2048]{1,0:T(8,128)(2,1)S(1)}, bf16[16,2048]{1,0:T(8,128)(2,1)S(1)}, u32[]{:S(2)}, u32[]{:S(2)}) collective-permute-start(bf16[16,2048]{1,0:T(8,128)(2,1)S(1)} %get-tuple-element.51), channel_id=1, source_target_pairs={{0,2},{1,3},{2,0},{3,1},{4,6},{5,7},{6,4},{7,5},{8,10},{9,11},{10,... | collective-permute-start | bytes 196616 | tf_op jit(solution)/shard_map/ppermute | solution.py:285
  35.0 10.1 %collective-permute-start.9 = (bf16[16,2048]{1,0:T(8,128)(2,1)S(1)}, bf16[16,2048]{1,0:T(8,128)(2,1)S(1)}, u32[]{:S(2)}, u32[]{:S(2)}) collective-permute-start(bf16[16,2048]{1,0:T(8,128)(2,1)S(1)} %get-tuple-element.52), channel_id=1, source_target_pairs={{0,4},{1,5},{2,6},{3,7},{4,0},{5,1},{6,2},{7,3},{8,12},{9,13},{10,... | collective-permute-start | bytes 196616 | tf_op jit(solution)/shard_map/ppermute | solution.py:285
  37.6 7.5 %collective-permute-start.10 = (bf16[16,2048]{1,0:T(8,128)(2,1)S(1)}, bf16[16,2048]{1,0:T(8,128)(2,1)S(1)}, u32[]{:S(2)}, u32[]{:S(2)}) collective-permute-start(bf16[16,2048]{1,0:T(8,128)(2,1)S(1)} %get-tuple-element.53), channel_id=1, source_target_pairs={{0,6},{1,7},{2,4},{3,5},{4,2},{5,3},{6,0},{7,1},{8,14},{9,15},{10,... | collective-permute-start | bytes 196616 | tf_op jit(solution)/shard_map/ppermute | solution.py:285
  39.0 8.7 %copy-start.1 = (bf16[2048,128]{1,0:T(8,128)(2,1)S(1)}, bf16[2048,128]{1,0:T(8,128)(2,1)}, u32[]{:S(2)}) copy-start(bf16[2048,128]{1,0:T(8,128)(2,1)} %refs_6_.1) | copy-start | bytes 1572868
  39.1 8.7 %copy-start.2 = (bf16[2048,128]{1,0:T(8,128)(2,1)S(1)}, bf16[2048,128]{1,0:T(8,128)(2,1)}, u32[]{:S(2)}) copy-start(bf16[2048,128]{1,0:T(8,128)(2,1)} %refs_7_.1) | copy-start | bytes 1572868
  39.1 8.7 %copy-start.3 = (f32[2048]{0:T(1024)S(1)}, f32[2048]{0:T(1024)}, u32[]{:S(2)}) copy-start(f32[2048]{0:T(1024)} %param.13) | copy-start | bytes 24580
  39.1 6.9 %collective-permute-start.15 = (bf16[96,128]{1,0:T(8,128)(2,1)S(1)}, bf16[96,128]{1,0:T(8,128)(2,1)S(1)}, u32[]{:S(2)}, u32[]{:S(2)}) collective-permute-start(bf16[96,128]{1,0:T(8,128)(2,1)S(1)} %get-tuple-element.62), channel_id=1, source_target_pairs={{0,2},{1,3},{2,0},{3,1},{4,6},{5,7},{6,4},{7,5},{8,10},{9,11},{10,... | collective-permute-start | bytes 73736 | tf_op jit(solution)/shard_map/ppermute | solution.py:285
  39.2 6.8 %collective-permute-start.16 = (bf16[96,128]{1,0:T(8,128)(2,1)S(1)}, bf16[96,128]{1,0:T(8,128)(2,1)S(1)}, u32[]{:S(2)}, u32[]{:S(2)}) collective-permute-start(bf16[96,128]{1,0:T(8,128)(2,1)S(1)} %get-tuple-element.63), channel_id=1, source_target_pairs={{0,4},{1,5},{2,6},{3,7},{4,0},{5,1},{6,2},{7,3},{8,12},{9,13},{10,... | collective-permute-start | bytes 73736 | tf_op jit(solution)/shard_map/ppermute | solution.py:285
  42.2 5.6 %collective-permute-start.17 = (bf16[96,128]{1,0:T(8,128)(2,1)S(1)}, bf16[96,128]{1,0:T(8,128)(2,1)S(1)}, u32[]{:S(2)}, u32[]{:S(2)}) collective-permute-start(bf16[96,128]{1,0:T(8,128)(2,1)S(1)} %get-tuple-element.64), channel_id=1, source_target_pairs={{0,6},{1,7},{2,4},{3,5},{4,2},{5,3},{6,0},{7,1},{8,14},{9,15},{10,... | collective-permute-start | bytes 73736 | tf_op jit(solution)/shard_map/ppermute | solution.py:285
where the time goes:
time: 49.2 us; the launch traced here: 49.1 us
  starting transfers between devices  22.9 us (47%)
  Pallas kernels  13.7 us (28%)
  waiting for transfers between devices  11.6 us (24%)
  between operations  0.78 us (2%)
    ppermute x21, starting transfers between devices, swap(): return lax.ppermute(value, axis, [(i, i ^ offset) for i in range(count)])  22.9 us
    ppermute x21, waiting for transfers between devices, swap(): return lax.ppermute(value, axis, [(i, i ^ offset) for i in range(count)])  11.6 us
    pallas_call x1, Pallas kernels, on_device(): call(functools.partial(target_kernel, t_blocks, t_own), [shape((lanes, HE...  3.1 us
    pallas_call x1, Pallas kernels, on_device(): call(functools.partial(far_kernel, s_half, sp_count), [shape((q_width, t_...  2.7 us
    pallas_call x1, Pallas kernels, on_device(): call(functools.partial(source_kernel, s_blocks, t_blocks, s_own, sp_count...  2.31 us
    pallas_call x1, Pallas kernels, on_device(): call(functools.partial(grad_out_kernel, 2 * s_half, sp_count), shape((q_w...  1.57 us
    pallas_call x1, Pallas kernels, on_device(): call(functools.partial(finish_source_kernel, z_count), shape((s_own, widt...  1.27 us
  transfers between devices with their start and end apart: 21, of which 4 were waited for; matrix products, arithmetic and copies ran while one was open for 0% of the time, Pallas kernels for 15%

commit v1 on v0

--- a/solution.py
+++ b/solution.py
@@ -63,7 +63,8 @@
 
 def block_offsets(blocks):
     half = max(blocks // 2, 1)
-    return [2 * (b % half) + b // half for b in range(blocks)]
+    near = [2 * z + (z > 0) for z in range(half)]
+    return (near + [off ^ 1 for off in near])[:blocks]
 
 
 def order_rows(rows, blocks):
@@ -89,45 +90,32 @@
     ]
 
 
-def source_kernel(
-    s_blocks, t_blocks, own, sp_count, source, cotangent, gain, w_key, w_value, *rest
-):
-    messages, rest = rest[:sp_count], rest[sp_count:]
-    part, held, held_c, weights, gains, sems, c_sems, w_sems = rest
-    copies = block_copies(source, held, sems, s_blocks)
-    c_copies = block_copies(cotangent, held_c, c_sems, t_blocks)
-    w_copies = [
+def source_kernel(blocks, own, source, gain, w_key, w_value, *rest):
+    message, part, held, weights, gains, sems, w_sems = rest
+    copies = block_copies(source, held, sems, blocks)
+    copies += [
         pltpu.make_async_copy(w, weights.at[:, pl.ds(n * HEAD, HEAD)], w_sems.at[n])
         for n, w in enumerate((w_key, w_value))
     ]
-    w_copies.append(pltpu.make_async_copy(gain, gains, w_sems.at[2]))
-    for copy in copies + w_copies + c_copies:
+    copies.append(pltpu.make_async_copy(gain, gains, w_sems.at[2]))
+    for copy in copies:
         copy.start()
-    for copy in copies + w_copies:
+    for copy in copies:
         copy.wait()
-    rows, c_rows = held.shape[0], held_c.shape[0]
+    rows = held.shape[0]
     wide = held[...].astype(F32)
     acc = nn((wide * gains[...]).astype(BF16), weights[...])
     both = (acc * inverse_rms(wide)).astype(BF16)
-    for message in messages:
-        message[0:rows, :] = both[:, 0:HEAD]
-        message[rows : 2 * rows, :] = both[:, HEAD:]
+    message[0:rows, :] = both[:, 0:HEAD]
+    message[rows:, :] = both[:, HEAD:]
     part[...] = held[0:own, :]
-    for copy in c_copies:
-        copy.wait()
-    pieces = held_c.shape[1] // (sp_count * HEAD)
-    sp_place = lax.axis_index("sp")
-    for k, message in enumerate(messages):
-        for piece in range(pieces):
-            column = pl.multiple_of(((sp_place ^ k) * pieces + piece) * HEAD, HEAD)
-            at = 2 * rows + piece * c_rows
-            message[at : at + c_rows, :] = held_c[:, pl.ds(column, HEAD)]
 
 
 def target_kernel(
-    blocks, own, target, cotangent, gain, w_query, w_out, q, q_t, da, da_t, part,
-    held_t, held_c, gains, weights, sems_t, sems_c, sems,
+    blocks, own, sp_count, target, cotangent, gain, w_query, w_out, q, q_t, da, da_t, part, *rest
 ):
+    cots, rest = rest[:sp_count], rest[sp_count:]
+    held_t, held_c, gains, weights, sems_t, sems_c, sems = rest
     t_copies = block_copies(target, held_t, sems_t, blocks)
     c_copies = block_copies(cotangent, held_c, sems_c, blocks)
     gain_copy = pltpu.make_async_copy(gain, gains, sems.at[0])
@@ -148,6 +136,14 @@
     part[...] = held_t[0:own, :]
     for copy in c_copies + [w_copy]:
         copy.wait()
+    pieces = held_c.shape[1] // (sp_count * HEAD)
+    sp_place = lax.axis_index("sp")
+    for k, cot in enumerate(cots):
+        for piece in range(pieces):
+            column = pl.multiple_of(((sp_place ^ k) * pieces + piece) * HEAD, HEAD)
+            cot[piece * rows // 2 : (piece + 1) * rows // 2, :] = held_c[
+                0 : rows // 2, pl.ds(column, HEAD)
+            ]
     grads = nt(held_c[...], weights[...]).astype(BF16)
     for h in range(heads):
         grad = grads[:, h * HEAD : (h + 1) * HEAD]
@@ -223,20 +219,32 @@
     return total
 
 
-def fold_core_kernel(keep, received, *outs):
+def fold_core_kernel(keep, received, *refs):
+    count = len(refs) // 2
+    for k, (cot, message) in enumerate(zip(refs[:count], refs[count:])):
+        rows = message.shape[0] - cot.shape[0]
+        span = slice(k * rows, (k + 1) * rows)
+        message[0:rows, :] = summed((keep, received), span).astype(BF16)
+        message[rows:, :] = cot[...]
+
+
+def fold_target_kernel(keep, received, *outs):
     step = keep.shape[0] // len(outs)
     for b, out in enumerate(outs):
         out[...] = summed((keep, received), slice(b * step, (b + 1) * step)).astype(BF16)
 
 
 def fold_sp_kernel(half, count, *refs):
-    parts, outs = refs[:count], refs[count:]
+    messages, cots, outs = refs[:count], refs[count], refs[count + 1 :]
     step = half // len(outs)
     for b, out in enumerate(outs):
         for part in range(2):
             at = part * half + b * step
-            total = summed(parts, slice(at, at + step))
+            total = summed(messages, slice(at, at + step))
             out[part * step : (part + 1) * step, :] = total.astype(BF16)
+    rows = cots.shape[0] // count
+    for k, message in enumerate(messages):
+        cots[k * rows : (k + 1) * rows, :] = message[2 * half :, :]
 
 
 def finish_source_kernel(count, *refs):
@@ -247,27 +255,22 @@
     out[...] = norm_back(rows[...], gain[...], pulled).astype(BF16)
 
 
-def finish_target_kernel(count, *refs):
-    parts, (rows, gain, out) = refs[:count], refs[count:]
-    out[...] = norm_back(rows[...], gain[...], summed(parts)).astype(BF16)
-
-
-def grad_out_kernel(skip_cot, count, *refs):
-    atts, near, far, (out, cots) = (
-        refs[:count], refs[count : 2 * count], refs[2 * count : 3 * count], refs[3 * count :]
-    )
-    pieces = out.shape[1] // HEAD
+def finish_target_kernel(count, z_count, *refs):
+    parts, (part, gain), refs = refs[:z_count], refs[z_count : z_count + 2], refs[z_count + 2 :]
+    atts, (near, far, grad_target, grad_out, cots) = refs[:count], refs[count:]
+    grad_target[...] = norm_back(part[...], gain[...], summed(parts)).astype(BF16)
+    pieces = grad_out.shape[1] // HEAD
     rows = cots.shape[0] // 2
-    total = jnp.zeros(out.shape, F32)
-    for att, pair in zip(atts, zip(near, far)):
-        for side, message in enumerate(pair):
-            for piece in range(pieces):
-                at = skip_cot + piece * rows
-                cots[side * rows : (side + 1) * rows, piece * HEAD : (piece + 1) * HEAD] = message[
-                    at : at + rows, :
-                ]
+    total = jnp.zeros(grad_out.shape, F32)
+    for k, att in enumerate(atts):
+        first, second = (near, far) if k == 0 else (far, near)
+        for piece in range(pieces):
+            at = (k * pieces + piece) * rows
+            column = slice(piece * HEAD, (piece + 1) * HEAD)
+            cots[0:rows, column] = first[at : at + rows, :]
+            cots[rows:, column] = second[at : at + rows, :]
         total = total + nn(att[...], cots[...])
-    out[...] = total.astype(BF16)
+    grad_out[...] = total.astype(BF16)
 
 
 def on_device(target, source, cotangent, target_gain, source_gain, w_query, w_key, w_value, w_out):
@@ -281,17 +284,22 @@
     lanes = heads * t_rows
     target_gain, source_gain = target_gain[None, :], source_gain[None, :]
 
-    def swap(value, axis, count, offset):
-        return lax.ppermute(value, axis, [(i, i ^ offset) for i in range(count)])
-
-    def to_sp(values):
-        return [values[0]] + [swap(values[k], "sp", sp_count, k) for k in range(1, sp_count)]
+    def swap(value, sp_offset, tp_offset):
+        pairs = [
+            (s * tp_count + t, (s ^ sp_offset) * tp_count + (t ^ tp_offset))
+            for s in range(sp_count)
+            for t in range(tp_count)
+        ]
+        return lax.ppermute(value, ("sp", "tp"), pairs)
+
+    def to_sp(values, other_core):
+        return [values[0]] + [swap(values[k], k, other_core) for k in range(1, sp_count)]
 
     def to_z(values):
-        return [values[0]] + [swap(values[k], "tp", tp_count, 2 * k) for k in range(1, z_count)]
+        return [values[0]] + [swap(values[k], 0, 2 * k + 1) for k in range(1, z_count)]
 
     def to_core(value):
-        return swap(value, "tp", tp_count, 1)
+        return swap(value, 0, 1)
 
     s_blocks = tp_count if s_own % ROW_TILE == 0 else 1
     t_blocks = tp_count if t_own % ROW_TILE == 0 else 1
@@ -303,26 +311,27 @@
     far_rows = sp_count * s_half
     cot_rows = width // sp_count // HEAD * t_half
 
-    *near, source_part = call(
-        functools.partial(source_kernel, s_blocks, t_blocks, s_own, sp_count),
-        [shape((2 * s_half + cot_rows, HEAD), BF16)] * sp_count + [shape((s_own, width), BF16)],
+    message, source_part = call(
+        functools.partial(source_kernel, s_blocks, s_own),
+        [shape((2 * s_half, HEAD), BF16), shape((s_own, width), BF16)],
         4 * s_half * width * HEAD, s_rows * width * 2 + 4 * width * HEAD,
-        [HBM] * 5,
+        [HBM] * 4,
         [
             pltpu.VMEM((s_half, width), BF16),
-            pltpu.VMEM((t_half, width), BF16),
             pltpu.VMEM((width, 2 * HEAD), BF16),
             pltpu.VMEM((1, width), F32),
-        ]
-        + [pltpu.SemaphoreType.DMA((n,)) for n in (s_blocks, t_blocks, 3)],
-    )(*map(in_hbm, (source, cotangent, source_gain, w_key, w_value)))
-    near = to_sp(near)
+            pltpu.SemaphoreType.DMA((s_blocks,)),
+            pltpu.SemaphoreType.DMA((3,)),
+        ],
+    )(*map(in_hbm, (source, source_gain, w_key, w_value)))
+    near = to_sp([message] * sp_count, 1)
     far = [to_core(message) for message in near]
 
-    q, q_t, da, da_t, target_part = call(
-        functools.partial(target_kernel, t_blocks, t_own),
+    q, q_t, da, da_t, target_part, *cots = call(
+        functools.partial(target_kernel, t_blocks, t_own, sp_count),
         [shape((lanes, HEAD), BF16), shape((HEAD, lanes), BF16)] * 2
-        + [shape((t_own, width), BF16)],
+        + [shape((t_own, width), BF16)]
+        + [shape((cot_rows, HEAD), BF16)] * sp_count,
         4 * t_rows * width * q_width, 4 * width * q_width + 4 * t_rows * width,
         [HBM, HBM, HBM, VMEM, HBM],
         [pltpu.VMEM((t_rows, width), BF16)] * 2
@@ -356,16 +365,16 @@
         [VMEM, VMEM], (),
     )(dq, w_query)
     t_received = to_core(t_send)
-    grads = call(
-        fold_core_kernel, [shape((2 * s_half, HEAD), BF16)] * sp_count,
-        2 * far_rows * HEAD, 16 * far_rows * HEAD, [VMEM] * 2, (),
-    )(keep, received)
-    atts = to_sp([att_t] * sp_count)
-    grads = to_sp(grads)
+    messages = call(
+        fold_core_kernel, [shape((2 * s_half + cot_rows, HEAD), BF16)] * sp_count,
+        2 * far_rows * HEAD, 16 * far_rows * HEAD, [VMEM] * (2 + sp_count), (),
+    )(keep, received, *cots)
+    messages = to_sp(messages, 1)
+    atts = to_sp([att_t] * sp_count, 0)
 
     pieces = z_count if t_blocks > 1 else 1
     t_parts = call(
-        fold_core_kernel, [shape((t_half // pieces, width), BF16)] * pieces,
+        fold_target_kernel, [shape((t_half // pieces, width), BF16)] * pieces,
         t_half * width, 8 * t_half * width, [VMEM] * 2, (),
     )(t_keep, t_received)
     if t_blocks == 1:
@@ -373,26 +382,24 @@
     t_parts = to_z(t_parts)
 
     pieces = z_count if s_blocks > 1 else 1
-    s_parts = call(
+    cots, *s_parts = call(
         functools.partial(fold_sp_kernel, s_half, sp_count),
-        [shape((2 * s_half // pieces, HEAD), BF16)] * pieces,
+        [shape((sp_count * cot_rows, HEAD), BF16)]
+        + [shape((2 * s_half // pieces, HEAD), BF16)] * pieces,
         2 * s_half * HEAD * sp_count, 16 * s_half * HEAD, [VMEM] * sp_count, (),
-    )(*grads)
+    )(*messages)
     if s_blocks == 1:
         both = s_parts[0].reshape(2, z_count, s_own, HEAD)
         s_parts = [both[:, b].reshape(2 * s_own, HEAD) for b in range(z_count)]
     s_parts = to_z(s_parts)
-
-    grad_target = call(
-        functools.partial(finish_target_kernel, z_count), shape((t_own, width), BF16),
-        10 * t_own * width, 8 * t_own * width, [VMEM] * (z_count + 2), (),
-    )(*t_parts, target_part, target_gain)
-    grad_out = call(
-        functools.partial(grad_out_kernel, 2 * s_half, sp_count),
-        shape((q_width, width // sp_count), BF16),
-        2 * q_width * width * t_rows, 2 * q_width * width, [VMEM] * (3 * sp_count),
+    far_cots = to_core(cots)
+
+    grad_target, grad_out = call(
+        functools.partial(finish_target_kernel, sp_count, z_count),
+        [shape((t_own, width), BF16), shape((q_width, width // sp_count), BF16)],
+        2 * q_width * width * t_rows, 2 * q_width * width, [VMEM] * (z_count + sp_count + 4),
         [pltpu.VMEM((t_rows, width // sp_count), BF16)],
-    )(*atts, *near, *far)
+    )(*t_parts, target_part, target_gain, *atts, cots, far_cots)
     grad_source = call(
         functools.partial(finish_source_kernel, z_count), shape((s_own, width), BF16),
         4 * s_own * width * HEAD, 4 * width * HEAD, [VMEM] * (z_count + 4), (),

time: 49.2 us -> 56.9 us (1.16)
  waiting for transfers between devices: 11.6 us -> 22.6 us
  starting transfers between devices: 22.9 us -> 20.7 us
  Pallas kernels: 13.7 us -> 12.7 us
    ppermute x21 -> x22, waiting for transfers between devices: 11.6 us -> 22.6 us  [swap(): return lax.ppermute(value, ('sp', 'tp'), pairs)]
    ppermute x21 -> x22, starting transfers between devices: 22.9 us -> 20.7 us  [swap(): return lax.ppermute(value, ('sp', 'tp'), pairs)]
    pallas_call x7 -> x6, Pallas kernels: 8.01 us -> 6.98 us  [the longest x1 3.13 us: on_device(): call(functools.partial(target_kernel, t_blocks, t_own, sp_count), [shape(...]
  transfers between devices with their start and end apart: 21 -> 22, of which waited for: 4 -> 12; matrix products, arithmetic and copies ran while one was open for 0% -> 0% of each run, Pallas kernels for 15% -> 11%
where the time goes in v1:
time: 56.9 us; the launch traced here: 56.7 us
  waiting for transfers between devices  22.6 us (40%)
  starting transfers between devices  20.7 us (36%)
  Pallas kernels  12.7 us (22%)
  between operations  0.76 us (1%)
    ppermute x22, waiting for transfers between devices, swap(): return lax.ppermute(value, ('sp', 'tp'), pairs)  22.6 us
    ppermute x22, starting transfers between devices, swap(): return lax.ppermute(value, ('sp', 'tp'), pairs)  20.7 us
    pallas_call x1, Pallas kernels, on_device(): call(functools.partial(target_kernel, t_blocks, t_own, sp_count), [shape(...  3.13 us
    pallas_call x1, Pallas kernels, on_device(): call(functools.partial(far_kernel, s_half, sp_count), [shape((q_width, t_...  2.68 us
    pallas_call x1, Pallas kernels, on_device(): call(functools.partial(source_kernel, s_blocks, s_own), [shape((2 * s_hal...  2.1 us
    pallas_call x1, Pallas kernels, on_device(): call(functools.partial(finish_target_kernel, sp_count, z_count), [shape((...  1.57 us
    pallas_call x1, Pallas kernels, on_device(): call(functools.partial(finish_source_kernel, z_count), shape((s_own, widt...  1.27 us
  transfers between devices with their start and end apart: 22, of which 12 were waited for; matrix products, arithmetic and copies ran while one was open for 0% of the time, Pallas kernels for 11%

profile of v1, /device:TPU:0, one launch (start us, length us, event | category | flops | bytes accessed | tf_op | source)
XLA Modules:
  0.0 56.7 jit_solution(10302463579467390169)
XLA Ops:
  0.6 2.1 %shard_map.113 = (bf16[384,128]{1,0:T(8,128)(2,1)S(1)}, bf16[48,2048]{1,0:T(8,128)(2,1)S(1)}) custom-call(bf16[384,2048]{1,0:T(8,128)(2,1)} %source.1, f32[1,2048]{1,0:T(1,128)} %bitcast.2, bf16[2048,128]{1,0:T(8,128)(2,1)} %refs_6_.1, bf16[2048,128]{1,0:T(8,128)(2,1)} %refs_7_.1), custom_call_target="tpu_custom_call" | custom-call | flops 201326592 | bytes 2621440 | tf_op jit(solution)/shard_map/pallas_call | solution.py:314
  2.7 3.4 %collective-permute-start.2 = (bf16[384,128]{1,0:T(8,128)(2,1)S(1)}, bf16[384,128]{1,0:T(8,128)(2,1)S(1)}, u32[]{:S(2)}, u32[]{:S(2)}) collective-permute-start(bf16[384,128]{1,0:T(8,128)(2,1)S(1)} %get-tuple-element.43.rest_0_), channel_id=1, source_target_pairs={{0,25},{1,24},{2,27},{3,26},{4,29},{5,28},{6,31},{7,30},{8,17},{9,... | collective-permute-start | bytes 294920 | tf_op jit(solution)/shard_map/ppermute | solution.py:293
  6.2 0.8 %collective-permute-start.1 = (bf16[384,128]{1,0:T(8,128)(2,1)S(1)}, bf16[384,128]{1,0:T(8,128)(2,1)S(1)}, u32[]{:S(2)}, u32[]{:S(2)}) collective-permute-start(bf16[384,128]{1,0:T(8,128)(2,1)S(1)} %get-tuple-element.43.rest_0_), channel_id=1, source_target_pairs={{0,17},{1,16},{2,19},{3,18},{4,21},{5,20},{6,23},{7,22},{8,25},{9,... | collective-permute-start | bytes 294920 | tf_op jit(solution)/shard_map/ppermute | solution.py:293
  7.0 0.1 collective-permute-start
  7.1 0.0 collective-permute-start.3
  7.1 2.3 %collective-permute-done.2.rest_3_ = bf16[384,128]{1,0:T(8,128)(2,1)S(1)} collective-permute-done((bf16[384,128]{1,0:T(8,128)(2,1)S(1)}, bf16[384,128]{1,0:T(8,128)(2,1)S(1)}, u32[]{:S(2)}, u32[]{:S(2)}) %collective-permute-start.2) | collective-permute-done | bytes 98336 | tf_op jit(solution)/shard_map/ppermute | solution.py:293
  9.4 0.1 collective-permute-start.6
  9.5 1.9 %collective-permute-done.1.rest_2_ = bf16[384,128]{1,0:T(8,128)(2,1)S(1)} collective-permute-done((bf16[384,128]{1,0:T(8,128)(2,1)S(1)}, bf16[384,128]{1,0:T(8,128)(2,1)S(1)}, u32[]{:S(2)}, u32[]{:S(2)}) %collective-permute-start.1) | collective-permute-done | bytes 98336 | tf_op jit(solution)/shard_map/ppermute | solution.py:293
  11.4 0.3 collective-permute-start.5
  11.8 0.7 %collective-permute-done.rest_1_ = bf16[384,128]{1,0:T(8,128)(2,1)S(1)} collective-permute-done((bf16[384,128]{1,0:T(8,128)(2,1)S(1)}, bf16[384,128]{1,0:T(8,128)(2,1)S(1)}, u32[]{:S(2)}, u32[]{:S(2)}) %collective-permute-start) | collective-permute-done | bytes 98336 | tf_op jit(solution)/shard_map/ppermute | solution.py:293
  12.5 0.1 collective-permute-start.4
  12.6 3.1 %shard_map.112 = (bf16[512,128]{1,0:T(8,128)(2,1)S(1)}, bf16[128,512]{1,0:T(8,128)(2,1)S(1)}, bf16[512,128]{1,0:T(8,128)(2,1)S(1)}, bf16[128,512]{1,0:T(8,128)(2...) custom-call(bf16[128,2048]{1,0:T(8,128)(2,1)} %target.1, ...), custom_call_target="tpu_custom_call" | custom-call | flops 536870912 | bytes 5242880 | tf_op jit(solution)/shard_map/pallas_call | solution.py:330
  15.7 1.0 %shard_map.114 = (f32[768,512]{1,0:T(8,128)S(1)}, f32[768,512]{1,0:T(8,128)S(1)}, f32[1,512]{1,0:T(1,128)S(1)}, f32[128,512]{1,0:T(8,128)S(1)}) custom-call(bf16[128,512]{1,0:T(8,128)(2,1)S(1)} %get-tuple-element.40.q_t, bf16[128,512]{1,0:T(8,128)(2,1)S(1)} %get-tuple-element.42.da_t, bf16[384,128]{1,0:T(8,128)(2,1)S(1)} %get-tuple-element.43.rest_0_, ...), custom_call_target="tpu_custom_call" | custom-call | flops 301989888 | bytes 3145728 | tf_op jit(solution)/shard_map/pallas_call | solution.py:342
  16.7 0.0 collective-permute-done.3.rest_4_
  16.7 0.0 collective-permute-done.6.rest_7_
  16.7 0.0 collective-permute-done.5.rest_6_
  16.7 2.7 %shard_map.115 = (bf16[512,128]{1,0:T(8,128)(2,1)S(1)}, bf16[128,512]{1,0:T(8,128)(2,1)S(1)}, f32[1536,128]{1,0:T(8,128)S(1)}, bf16[1536,128]{1,0:T(8,128)(2,1)S(1)}) custom-call(bf16[512,128]{1,0:T(8,128)(2,1)S(1)} %get-tuple-element.39.q, bf16[128,512]{1,0:T(8,128)(2,1)S(1)} %get-tuple-element.40.q_t, bf16[512,128]{1,0:T(8,128)(2,1)S(1)} %get-tuple-element.41.da, ...), custom_call_target="tpu_custom_call" | custom-call | flops 905969664 | bytes 3145728 | tf_op jit(solution)/shard_map/pallas_call | solution.py:348
  19.4 0.5 collective-permute-start.14
  19.9 1.3 %collective-permute-done.14.received = bf16[1536,128]{1,0:T(8,128)(2,1)S(1)} collective-permute-done((bf16[1536,128]{1,0:T(8,128)(2,1)S(1)}, bf16[1536,128]{1,0:T(8,128)(2,1)S(1)}, u32[]{:S(2)}, u32[]{:S(2)}) %collective-permute-start.14) | collective-permute-done | bytes 393248 | tf_op jit(solution)/shard_map/ppermute | solution.py:293
  21.2 0.1 shard_map.118
  21.3 1.6 %collective-permute-start.15 = (bf16[640,128]{1,0:T(8,128)(2,1)S(1)}, bf16[640,128]{1,0:T(8,128)(2,1)S(1)}, u32[]{:S(2)}, u32[]{:S(2)}) collective-permute-start(bf16[640,128]{1,0:T(8,128)(2,1)S(1)} %get-tuple-element.64), channel_id=1, source_target_pairs={{0,9},{1,8},{2,11},{3,10},{4,13},{5,12},{6,15},{7,14},{8,1},{9,0},... | collective-permute-start | bytes 491528 | tf_op jit(solution)/shard_map/ppermute | solution.py:293
  22.9 0.7 %collective-permute-start.16 = (bf16[640,128]{1,0:T(8,128)(2,1)S(1)}, bf16[640,128]{1,0:T(8,128)(2,1)S(1)}, u32[]{:S(2)}, u32[]{:S(2)}) collective-permute-start(bf16[640,128]{1,0:T(8,128)(2,1)S(1)} %get-tuple-element.65), channel_id=1, source_target_pairs={{0,17},{1,16},{2,19},{3,18},{4,21},{5,20},{6,23},{7,22},{8,25},{9,... | collective-permute-start | bytes 491528 | tf_op jit(solution)/shard_map/ppermute | solution.py:293
  23.6 1.0 %collective-permute-start.17 = (bf16[640,128]{1,0:T(8,128)(2,1)S(1)}, bf16[640,128]{1,0:T(8,128)(2,1)S(1)}, u32[]{:S(2)}, u32[]{:S(2)}) collective-permute-start(bf16[640,128]{1,0:T(8,128)(2,1)S(1)} %get-tuple-element.66), channel_id=1, source_target_pairs={{0,25},{1,24},{2,27},{3,26},{4,29},{5,28},{6,31},{7,30},{8,17},{9,... | collective-permute-start | bytes 491528 | tf_op jit(solution)/shard_map/ppermute | solution.py:293
  24.6 0.8 %shard_map.116 = (f32[64,2048]{1,0:T(8,128)S(1)}, bf16[64,2048]{1,0:T(8,128)(2,1)S(1)}) custom-call(bf16[128,512]{1,0:T(8,128)(2,1)S(1)} %get-tuple-element.48.dq, bf16[2048,512]{1,0:T(8,128)(2,1)S(1)} %copy-done), custom_call_target="tpu_custom_call" | custom-call | flops 268435456 | bytes 4194304 | tf_op jit(solution)/shard_map/pallas_call | solution.py:361
  25.4 0.0 copy-start.4
  25.4 0.2 collective-permute-start.7
  25.6 1.9 %collective-permute-done.15.refs_1_ = bf16[640,128]{1,0:T(8,128)(2,1)S(1)} collective-permute-done((bf16[640,128]{1,0:T(8,128)(2,1)S(1)}, bf16[640,128]{1,0:T(8,128)(2,1)S(1)}, u32[]{:S(2)}, u32[]{:S(2)}) %collective-permute-start.15) | collective-permute-done | bytes 163872 | tf_op jit(solution)/shard_map/ppermute | solution.py:293
  27.5 3.6 %collective-permute-done.16.refs_2_ = bf16[640,128]{1,0:T(8,128)(2,1)S(1)} collective-permute-done((bf16[640,128]{1,0:T(8,128)(2,1)S(1)}, bf16[640,128]{1,0:T(8,128)(2,1)S(1)}, u32[]{:S(2)}, u32[]{:S(2)}) %collective-permute-start.16) | collective-permute-done | bytes 163872 | tf_op jit(solution)/shard_map/ppermute | solution.py:293
  31.1 1.2 %collective-permute-done.17.refs_3_ = bf16[640,128]{1,0:T(8,128)(2,1)S(1)} collective-permute-done((bf16[640,128]{1,0:T(8,128)(2,1)S(1)}, bf16[640,128]{1,0:T(8,128)(2,1)S(1)}, u32[]{:S(2)}, u32[]{:S(2)}) %collective-permute-start.17) | collective-permute-done | bytes 163872 | tf_op jit(solution)/shard_map/ppermute | solution.py:293
  32.4 0.1 shard_map.119
  32.4 0.4 collective-permute-start.18
  32.9 1.4 %collective-permute-start.13 = (bf16[512,128]{1,0:T(8,128)(2,1)S(1)}, bf16[512,128]{1,0:T(8,128)(2,1)S(1)}, u32[]{:S(2)}, u32[]{:S(2)}) collective-permute-start(bf16[512,128]{1,0:T(8,128)(2,1)S(1)} %get-tuple-element.56.refs_6_), channel_id=1, source_target_pairs={{0,24},{1,25},{2,26},{3,27},{4,28},{5,29},{6,30},{7,31},{8,16},{9,... | collective-permute-start | bytes 393224 | tf_op jit(solution)/shard_map/ppermute | solution.py:293
  34.3 0.5 collective-permute-start.12
  34.8 1.5 %collective-permute-start.11 = (bf16[512,128]{1,0:T(8,128)(2,1)S(1)}, bf16[512,128]{1,0:T(8,128)(2,1)S(1)}, u32[]{:S(2)}, u32[]{:S(2)}) collective-permute-start(bf16[512,128]{1,0:T(8,128)(2,1)S(1)} %get-tuple-element.56.refs_6_), channel_id=1, source_target_pairs={{0,8},{1,9},{2,10},{3,11},{4,12},{5,13},{6,14},{7,15},{8,0},{9,1},... | collective-permute-start | bytes 393224 | tf_op jit(solution)/shard_map/ppermute | solution.py:293
  36.3 3.8 %collective-permute-done.13.refs_9_ = bf16[512,128]{1,0:T(8,128)(2,1)S(1)} collective-permute-done((bf16[512,128]{1,0:T(8,128)(2,1)S(1)}, bf16[512,128]{1,0:T(8,128)(2,1)S(1)}, u32[]{:S(2)}, u32[]{:S(2)}) %collective-permute-start.13) | collective-permute-done | bytes 131104 | tf_op jit(solution)/shard_map/ppermute | solution.py:293
  40.2 0.0 collective-permute-start.19
  40.2 1.9 %collective-permute-done.12.refs_8_ = bf16[512,128]{1,0:T(8,128)(2,1)S(1)} collective-permute-done((bf16[512,128]{1,0:T(8,128)(2,1)S(1)}, bf16[512,128]{1,0:T(8,128)(2,1)S(1)}, u32[]{:S(2)}, u32[]{:S(2)}) %collective-permute-start.12) | collective-permute-done | bytes 131104 | tf_op jit(solution)/shard_map/ppermute | solution.py:293
  42.1 2.2 %collective-permute-start.20 = (bf16[96,128]{1,0:T(8,128)(2,1)S(1)}, bf16[96,128]{1,0:T(8,128)(2,1)S(1)}, u32[]{:S(2)}, u32[]{:S(2)}) collective-permute-start(bf16[96,128]{1,0:T(8,128)(2,1)S(1)} %get-tuple-element.71), channel_id=1, source_target_pairs={{0,5},{1,4},{2,7},{3,6},{4,1},{5,0},{6,3},{7,2},{8,13},{9,12},{10,... | collective-permute-start | bytes 73736 | tf_op jit(solution)/shard_map/ppermute | solution.py:293
  44.3 1.4 %collective-permute-start.21 = (bf16[96,128]{1,0:T(8,128)(2,1)S(1)}, bf16[96,128]{1,0:T(8,128)(2,1)S(1)}, u32[]{:S(2)}, u32[]{:S(2)}) collective-permute-start(bf16[96,128]{1,0:T(8,128)(2,1)S(1)} %get-tuple-element.72), channel_id=1, source_target_pairs={{0,7},{1,6},{2,5},{3,4},{4,3},{5,2},{6,1},{7,0},{8,15},{9,14},{10,... | collective-permute-start | bytes 73736 | tf_op jit(solution)/shard_map/ppermute | solution.py:293
  45.8 0.3 collective-permute-start.8
  46.1 0.2 collective-permute-done.20.refs_2_
  46.3 2.4 %collective-permute-start.9 = (bf16[16,2048]{1,0:T(8,128)(2,1)S(1)}, bf16[16,2048]{1,0:T(8,128)(2,1)S(1)}, u32[]{:S(2)}, u32[]{:S(2)}) collective-permute-start(bf16[16,2048]{1,0:T(8,128)(2,1)S(1)} %get-tuple-element.53), channel_id=1, source_target_pairs={{0,5},{1,4},{2,7},{3,6},{4,1},{5,0},{6,3},{7,2},{8,13},{9,12},{10,... | collective-permute-start | bytes 196616 | tf_op jit(solution)/shard_map/ppermute | solution.py:293
  48.7 0.8 %collective-permute-done.21.refs_3_ = bf16[96,128]{1,0:T(8,128)(2,1)S(1)} collective-permute-done((bf16[96,128]{1,0:T(8,128)(2,1)S(1)}, bf16[96,128]{1,0:T(8,128)(2,1)S(1)}, u32[]{:S(2)}, u32[]{:S(2)}) %collective-permute-start.21) | collective-permute-done | bytes 24608 | tf_op jit(solution)/shard_map/ppermute | solution.py:293
  49.5 1.6 %collective-permute-start.10 = (bf16[16,2048]{1,0:T(8,128)(2,1)S(1)}, bf16[16,2048]{1,0:T(8,128)(2,1)S(1)}, u32[]{:S(2)}, u32[]{:S(2)}) collective-permute-start(bf16[16,2048]{1,0:T(8,128)(2,1)S(1)} %get-tuple-element.54), channel_id=1, source_target_pairs={{0,7},{1,6},{2,5},{3,4},{4,3},{5,2},{6,1},{7,0},{8,15},{9,14},{10,... | collective-permute-start | bytes 196616 | tf_op jit(solution)/shard_map/ppermute | solution.py:293
  51.1 1.3 %shard_map.121 = bf16[48,2048]{1,0:T(8,128)(2,1)} custom-call(bf16[96,128]{1,0:T(8,128)(2,1)S(1)} %get-tuple-element.69.refs_0_, bf16[96,128]{1,0:T(8,128)(2,1)S(1)} %collective-permute-done.19.refs_1_, bf16[96,128]{1,0:T(8,128)(2,1)S(1)} %collective-permute-done.20.refs_2_, bf16[96,128]{1,0:T(8,128)(2,1)S(1)} %collective-permute-done.21.refs_3_, ...), custom_call_target="tpu_custom_call" | custom-call | flops 50331648 | bytes 1048576 | tf_op jit(solution)/shard_map/pallas_call | solution.py:403
  52.4 2.8 %collective-permute-done.10.refs_3_ = bf16[16,2048]{1,0:T(8,128)(2,1)S(1)} collective-permute-done((bf16[16,2048]{1,0:T(8,128)(2,1)S(1)}, bf16[16,2048]{1,0:T(8,128)(2,1)S(1)}, u32[]{:S(2)}, u32[]{:S(2)}) %collective-permute-start.10) | collective-permute-done | bytes 65568 | tf_op jit(solution)/shard_map/ppermute | solution.py:293
  55.1 0.0 collective-permute-done.18.refs_11_
  55.1 1.6 %shard_map.120 = (bf16[16,2048]{1,0:T(8,128)(2,1)}, bf16[512,512]{1,0:T(8,128)(2,1)}) custom-call(bf16[16,2048]{1,0:T(8,128)(2,1)S(1)} %get-tuple-element.51.refs_0_, bf16[16,2048]{1,0:T(8,128)(2,1)S(1)} %collective-permute-done.8.refs_1_, bf16[16,2048]{1,0:T(8,128)(2,1)S(1)} %collective-permute-done.9.refs_2_, ...), custom_call_target="tpu_custom_call" | custom-call | flops 268435456 | bytes 2097152 | tf_op jit(solution)/shard_map/pallas_call | solution.py:397
  (16 shorter events, 0.1 us)
Async XLA Ops:
  0.6 12.0 %copy-start = (bf16[2048,512]{1,0:T(8,128)(2,1)S(1)}, bf16[2048,512]{1,0:T(8,128)(2,1)}, u32[]{:S(2)}) copy-start(bf16[2048,512]{1,0:T(8,128)(2,1)} %w_query.3) | copy-start | bytes 6291460
  2.7 6.7 %collective-permute-start.2 = (bf16[384,128]{1,0:T(8,128)(2,1)S(1)}, bf16[384,128]{1,0:T(8,128)(2,1)S(1)}, u32[]{:S(2)}, u32[]{:S(2)}) collective-permute-start(bf16[384,128]{1,0:T(8,128)(2,1)S(1)} %get-tuple-element.43.rest_0_), channel_id=1, source_target_pairs={{0,25},{1,24},{2,27},{3,26},{4,29},{5,28},{6,31},{7,30},{8,17},{9,... | collective-permute-start | bytes 294920 | tf_op jit(solution)/shard_map/ppermute | solution.py:293
  6.2 5.3 %collective-permute-start.1 = (bf16[384,128]{1,0:T(8,128)(2,1)S(1)}, bf16[384,128]{1,0:T(8,128)(2,1)S(1)}, u32[]{:S(2)}, u32[]{:S(2)}) collective-permute-start(bf16[384,128]{1,0:T(8,128)(2,1)S(1)} %get-tuple-element.43.rest_0_), channel_id=1, source_target_pairs={{0,17},{1,16},{2,19},{3,18},{4,21},{5,20},{6,23},{7,22},{8,25},{9,... | collective-permute-start | bytes 294920 | tf_op jit(solution)/shard_map/ppermute | solution.py:293
  7.0 5.5 %collective-permute-start = (bf16[384,128]{1,0:T(8,128)(2,1)S(1)}, bf16[384,128]{1,0:T(8,128)(2,1)S(1)}, u32[]{:S(2)}, u32[]{:S(2)}) collective-permute-start(bf16[384,128]{1,0:T(8,128)(2,1)S(1)} %get-tuple-element.43.rest_0_), channel_id=1, source_target_pairs={{0,9},{1,8},{2,11},{3,10},{4,13},{5,12},{6,15},{7,14},{8,1},{9,0},... | collective-permute-start | bytes 294920 | tf_op jit(solution)/shard_map/ppermute | solution.py:293
  7.1 9.6 %collective-permute-start.3 = (bf16[384,128]{1,0:T(8,128)(2,1)S(1)}, bf16[384,128]{1,0:T(8,128)(2,1)S(1)}, u32[]{:S(2)}, u32[]{:S(2)}) collective-permute-start(bf16[384,128]{1,0:T(8,128)(2,1)S(1)} %get-tuple-element.43.rest_0_), channel_id=1, source_target_pairs={{0,1},{1,0},{2,3},{3,2},{4,5},{5,4},{6,7},{7,6},{8,9},{9,8},{10,11... | collective-permute-start | bytes 294920 | tf_op jit(solution)/shard_map/ppermute | solution.py:293
  9.4 7.3 %collective-permute-start.6 = (bf16[384,128]{1,0:T(8,128)(2,1)S(1)}, bf16[384,128]{1,0:T(8,128)(2,1)S(1)}, u32[]{:S(2)}, u32[]{:S(2)}) collective-permute-start(bf16[384,128]{1,0:T(8,128)(2,1)S(1)} %collective-permute-done.2.rest_3_), channel_id=1, source_target_pairs={{0,1},{1,0},{2,3},{3,2},{4,5},{5,4},{6,7},{7,6},{8,9},{9,8},{10,11... | collective-permute-start | bytes 294920 | tf_op jit(solution)/shard_map/ppermute | solution.py:293
  11.4 5.3 %collective-permute-start.5 = (bf16[384,128]{1,0:T(8,128)(2,1)S(1)}, bf16[384,128]{1,0:T(8,128)(2,1)S(1)}, u32[]{:S(2)}, u32[]{:S(2)}) collective-permute-start(bf16[384,128]{1,0:T(8,128)(2,1)S(1)} %collective-permute-done.1.rest_2_), channel_id=1, source_target_pairs={{0,1},{1,0},{2,3},{3,2},{4,5},{5,4},{6,7},{7,6},{8,9},{9,8},{10,11... | collective-permute-start | bytes 294920 | tf_op jit(solution)/shard_map/ppermute | solution.py:293
  12.5 4.3 %collective-permute-start.4 = (bf16[384,128]{1,0:T(8,128)(2,1)S(1)}, bf16[384,128]{1,0:T(8,128)(2,1)S(1)}, u32[]{:S(2)}, u32[]{:S(2)}) collective-permute-start(bf16[384,128]{1,0:T(8,128)(2,1)S(1)} %collective-permute-done.rest_1_), channel_id=1, source_target_pairs={{0,1},{1,0},{2,3},{3,2},{4,5},{5,4},{6,7},{7,6},{8,9},{9,8},{10,11... | collective-permute-start | bytes 294920 | tf_op jit(solution)/shard_map/ppermute | solution.py:293
  19.4 1.8 %collective-permute-start.14 = (bf16[1536,128]{1,0:T(8,128)(2,1)S(1)}, bf16[1536,128]{1,0:T(8,128)(2,1)S(1)}, u32[]{:S(2)}, u32[]{:S(2)}) collective-permute-start(bf16[1536,128]{1,0:T(8,128)(2,1)S(1)} %get-tuple-element.58), channel_id=1, source_target_pairs={{0,1},{1,0},{2,3},{3,2},{4,5},{5,4},{6,7},{7,6},{8,9},{9,8},{10,11... | collective-permute-start | bytes 1179656 | tf_op jit(solution)/shard_map/ppermute | solution.py:293
  21.3 6.2 %collective-permute-start.15 = (bf16[640,128]{1,0:T(8,128)(2,1)S(1)}, bf16[640,128]{1,0:T(8,128)(2,1)S(1)}, u32[]{:S(2)}, u32[]{:S(2)}) collective-permute-start(bf16[640,128]{1,0:T(8,128)(2,1)S(1)} %get-tuple-element.64), channel_id=1, source_target_pairs={{0,9},{1,8},{2,11},{3,10},{4,13},{5,12},{6,15},{7,14},{8,1},{9,0},... | collective-permute-start | bytes 491528 | tf_op jit(solution)/shard_map/ppermute | solution.py:293
  22.9 8.2 %collective-permute-start.16 = (bf16[640,128]{1,0:T(8,128)(2,1)S(1)}, bf16[640,128]{1,0:T(8,128)(2,1)S(1)}, u32[]{:S(2)}, u32[]{:S(2)}) collective-permute-start(bf16[640,128]{1,0:T(8,128)(2,1)S(1)} %get-tuple-element.65), channel_id=1, source_target_pairs={{0,17},{1,16},{2,19},{3,18},{4,21},{5,20},{6,23},{7,22},{8,25},{9,... | collective-permute-start | bytes 491528 | tf_op jit(solution)/shard_map/ppermute | solution.py:293
  23.6 8.8 %collective-permute-start.17 = (bf16[640,128]{1,0:T(8,128)(2,1)S(1)}, bf16[640,128]{1,0:T(8,128)(2,1)S(1)}, u32[]{:S(2)}, u32[]{:S(2)}) collective-permute-start(bf16[640,128]{1,0:T(8,128)(2,1)S(1)} %get-tuple-element.66), channel_id=1, source_target_pairs={{0,25},{1,24},{2,27},{3,26},{4,29},{5,28},{6,31},{7,30},{8,17},{9,... | collective-permute-start | bytes 491528 | tf_op jit(solution)/shard_map/ppermute | solution.py:293
  24.6 26.5 %copy-start.1 = (bf16[2048,128]{1,0:T(8,128)(2,1)S(1)}, bf16[2048,128]{1,0:T(8,128)(2,1)}, u32[]{:S(2)}) copy-start(bf16[2048,128]{1,0:T(8,128)(2,1)} %refs_6_.1) | copy-start | bytes 1572868
  24.6 26.5 %copy-start.2 = (bf16[2048,128]{1,0:T(8,128)(2,1)S(1)}, bf16[2048,128]{1,0:T(8,128)(2,1)}, u32[]{:S(2)}) copy-start(bf16[2048,128]{1,0:T(8,128)(2,1)} %refs_7_.1) | copy-start | bytes 1572868
  24.6 26.5 %copy-start.3 = (f32[2048]{0:T(1024)S(1)}, f32[2048]{0:T(1024)}, u32[]{:S(2)}) copy-start(f32[2048]{0:T(1024)} %param.13) | copy-start | bytes 24580
  25.4 29.8 %copy-start.4 = (f32[2048]{0:T(1024)S(1)}, f32[2048]{0:T(1024)}, u32[]{:S(2)}) copy-start(f32[2048]{0:T(1024)} %param.12) | copy-start | bytes 24580
  25.4 18.9 %collective-permute-start.7 = (bf16[64,2048]{1,0:T(8,128)(2,1)S(1)}, bf16[64,2048]{1,0:T(8,128)(2,1)S(1)}, u32[]{:S(2)}, u32[]{:S(2)}) collective-permute-start(bf16[64,2048]{1,0:T(8,128)(2,1)S(1)} %get-tuple-element.50), channel_id=1, source_target_pairs={{0,1},{1,0},{2,3},{3,2},{4,5},{5,4},{6,7},{7,6},{8,9},{9,8},{10,11... | collective-permute-start | bytes 786440 | tf_op jit(solution)/shard_map/ppermute | solution.py:293
  32.4 22.7 %collective-permute-start.18 = (bf16[1024,128]{1,0:T(8,128)(2,1)S(1)}, bf16[1024,128]{1,0:T(8,128)(2,1)S(1)}, u32[]{:S(2)}, u32[]{:S(2)}) collective-permute-start(bf16[1024,128]{1,0:T(8,128)(2,1)S(1)} %get-tuple-element.67.refs_10_), channel_id=1, source_target_pairs={{0,1},{1,0},{2,3},{3,2},{4,5},{5,4},{6,7},{7,6},{8,9},{9,8},{10,11... | collective-permute-start | bytes 786440 | tf_op jit(solution)/shard_map/ppermute | solution.py:293
  32.9 7.3 %collective-permute-start.13 = (bf16[512,128]{1,0:T(8,128)(2,1)S(1)}, bf16[512,128]{1,0:T(8,128)(2,1)S(1)}, u32[]{:S(2)}, u32[]{:S(2)}) collective-permute-start(bf16[512,128]{1,0:T(8,128)(2,1)S(1)} %get-tuple-element.56.refs_6_), channel_id=1, source_target_pairs={{0,24},{1,25},{2,26},{3,27},{4,28},{5,29},{6,30},{7,31},{8,16},{9,... | collective-permute-start | bytes 393224 | tf_op jit(solution)/shard_map/ppermute | solution.py:293
  34.3 7.8 %collective-permute-start.12 = (bf16[512,128]{1,0:T(8,128)(2,1)S(1)}, bf16[512,128]{1,0:T(8,128)(2,1)S(1)}, u32[]{:S(2)}, u32[]{:S(2)}) collective-permute-start(bf16[512,128]{1,0:T(8,128)(2,1)S(1)} %get-tuple-element.56.refs_6_), channel_id=1, source_target_pairs={{0,16},{1,17},{2,18},{3,19},{4,20},{5,21},{6,22},{7,23},{8,24},{9,... | collective-permute-start | bytes 393224 | tf_op jit(solution)/shard_map/ppermute | solution.py:293
  34.8 17.6 %collective-permute-start.11 = (bf16[512,128]{1,0:T(8,128)(2,1)S(1)}, bf16[512,128]{1,0:T(8,128)(2,1)S(1)}, u32[]{:S(2)}, u32[]{:S(2)}) collective-permute-start(bf16[512,128]{1,0:T(8,128)(2,1)S(1)} %get-tuple-element.56.refs_6_), channel_id=1, source_target_pairs={{0,8},{1,9},{2,10},{3,11},{4,12},{5,13},{6,14},{7,15},{8,0},{9,1},... | collective-permute-start | bytes 393224 | tf_op jit(solution)/shard_map/ppermute | solution.py:293
  40.2 5.7 %collective-permute-start.19 = (bf16[96,128]{1,0:T(8,128)(2,1)S(1)}, bf16[96,128]{1,0:T(8,128)(2,1)S(1)}, u32[]{:S(2)}, u32[]{:S(2)}) collective-permute-start(bf16[96,128]{1,0:T(8,128)(2,1)S(1)} %get-tuple-element.70), channel_id=1, source_target_pairs={{0,3},{1,2},{2,1},{3,0},{4,7},{5,6},{6,5},{7,4},{8,11},{9,10},{10,... | collective-permute-start | bytes 73736 | tf_op jit(solution)/shard_map/ppermute | solution.py:293
  42.1 4.2 %collective-permute-start.20 = (bf16[96,128]{1,0:T(8,128)(2,1)S(1)}, bf16[96,128]{1,0:T(8,128)(2,1)S(1)}, u32[]{:S(2)}, u32[]{:S(2)}) collective-permute-start(bf16[96,128]{1,0:T(8,128)(2,1)S(1)} %get-tuple-element.71), channel_id=1, source_target_pairs={{0,5},{1,4},{2,7},{3,6},{4,1},{5,0},{6,3},{7,2},{8,13},{9,12},{10,... | collective-permute-start | bytes 73736 | tf_op jit(solution)/shard_map/ppermute | solution.py:293
  44.3 5.2 %collective-permute-start.21 = (bf16[96,128]{1,0:T(8,128)(2,1)S(1)}, bf16[96,128]{1,0:T(8,128)(2,1)S(1)}, u32[]{:S(2)}, u32[]{:S(2)}) collective-permute-start(bf16[96,128]{1,0:T(8,128)(2,1)S(1)} %get-tuple-element.72), channel_id=1, source_target_pairs={{0,7},{1,6},{2,5},{3,4},{4,3},{5,2},{6,1},{7,0},{8,15},{9,14},{10,... | collective-permute-start | bytes 73736 | tf_op jit(solution)/shard_map/ppermute | solution.py:293
  45.8 6.5 %collective-permute-start.8 = (bf16[16,2048]{1,0:T(8,128)(2,1)S(1)}, bf16[16,2048]{1,0:T(8,128)(2,1)S(1)}, u32[]{:S(2)}, u32[]{:S(2)}) collective-permute-start(bf16[16,2048]{1,0:T(8,128)(2,1)S(1)} %get-tuple-element.52), channel_id=1, source_target_pairs={{0,3},{1,2},{2,1},{3,0},{4,7},{5,6},{6,5},{7,4},{8,11},{9,10},{10,... | collective-permute-start | bytes 196616 | tf_op jit(solution)/shard_map/ppermute | solution.py:293
  46.3 6.1 %collective-permute-start.9 = (bf16[16,2048]{1,0:T(8,128)(2,1)S(1)}, bf16[16,2048]{1,0:T(8,128)(2,1)S(1)}, u32[]{:S(2)}, u32[]{:S(2)}) collective-permute-start(bf16[16,2048]{1,0:T(8,128)(2,1)S(1)} %get-tuple-element.53), channel_id=1, source_target_pairs={{0,5},{1,4},{2,7},{3,6},{4,1},{5,0},{6,3},{7,2},{8,13},{9,12},{10,... | collective-permute-start | bytes 196616 | tf_op jit(solution)/shard_map/ppermute | solution.py:293
  49.5 5.7 %collective-permute-start.10 = (bf16[16,2048]{1,0:T(8,128)(2,1)S(1)}, bf16[16,2048]{1,0:T(8,128)(2,1)S(1)}, u32[]{:S(2)}, u32[]{:S(2)}) collective-permute-start(bf16[16,2048]{1,0:T(8,128)(2,1)S(1)} %get-tuple-element.54), channel_id=1, source_target_pairs={{0,7},{1,6},{2,5},{3,4},{4,3},{5,2},{6,1},{7,0},{8,15},{9,14},{10,... | collective-permute-start | bytes 196616 | tf_op jit(solution)/shard_map/ppermute | solution.py:293

commit v2 on v1

--- a/solution.py
+++ b/solution.py
@@ -12,6 +12,7 @@
 NORM_EPS = 1e-06
 LOG2_E = 1.4426950408889634
 ROW_TILE = 16
+DEPTH = 256
 
 BF16 = jnp.bfloat16
 F32 = jnp.float32
@@ -151,65 +152,79 @@
         da_t[:, h * rows : (h + 1) * rows] = grad.T
 
 
-def attend_half(half, q_t, da_t, messages, exps, prob_grads, total, out_acc):
-    for k, message in enumerate(messages):
-        key, value = message[0:half, :], message[half : 2 * half, :]
-        exponent = jnp.exp2(nn(key, q_t[...]) * (HEAD ** (-0.5) * LOG2_E))
+def joined(messages, half, part):
+    return jnp.concatenate([m[part * half : (part + 1) * half, :] for m in messages])
+
+
+def chunk_spans(rows, half):
+    step = DEPTH if rows % DEPTH == 0 else half
+    return [slice(at, at + step) for at in range(0, rows, step)]
+
+
+def attend(half, q_t, da_t, messages, exps, prob_grads, total, out_acc):
+    keys, values = joined(messages, half, 0), joined(messages, half, 1)
+    for span in chunk_spans(keys.shape[0], half):
+        exponent = jnp.exp2(nn(keys[span], q_t[...]) * (HEAD ** (-0.5) * LOG2_E))
         total = total + jnp.sum(exponent, axis=0, keepdims=True)
-        exps[k * half : (k + 1) * half, :] = exponent
-        prob_grads[k * half : (k + 1) * half, :] = nn(value, da_t[...])
-        out_acc = out_acc + nn(value.T, exponent.astype(BF16))
+        exps[span, :] = exponent
+        prob_grads[span, :] = nn(values[span], da_t[...])
+        out_acc = out_acc + nn(values[span].T, exponent.astype(BF16))
     return total, out_acc
+
+
+def pull_back(half, q, da, messages, exps, prob_grads, inv_total, delta, out):
+    inv_root = HEAD ** (-0.5)
+    keys = joined(messages, half, 0)
+    rows = keys.shape[0]
+    acc = jnp.zeros((HEAD, q.shape[0]), F32)
+    for span in chunk_spans(rows, half):
+        probs = exps[span, :] * inv_total
+        score_grad = (probs * (prob_grads[span, :] - delta)).astype(BF16)
+        dkey = nn(score_grad, q[...]) * inv_root
+        out[span, :] = dkey.astype(out.dtype)
+        dvalue = nn(probs.astype(BF16), da[...])
+        out[rows + span.start : rows + span.stop, :] = dvalue.astype(out.dtype)
+        acc = acc + nn(keys[span].T, score_grad)
+    return acc
 
 
 def near_kernel(half, sp_count, q_t, da_t, *rest):
     messages, (exps, prob_grads, total, out_acc) = rest[:sp_count], rest[sp_count:]
-    total[...], out_acc[...] = attend_half(
+    total[...], out_acc[...] = attend(
         half, q_t, da_t, messages, exps, prob_grads,
         jnp.zeros(total.shape, F32), jnp.zeros(out_acc.shape, F32),
     )
 
 
-def far_kernel(half, sp_count, q, q_t, da, da_t, near_exps, near_grads, near_total, near_acc, *rest):
-    near, far, rest = rest[:sp_count], rest[sp_count : 2 * sp_count], rest[2 * sp_count :]
-    att_t, dq, keep, send, far_exps, far_grads = rest
-    lanes = q_t.shape[1]
-    rows = dq.shape[0]
-    heads = lanes // rows
-    inv_root = HEAD ** (-0.5)
-    total, out_acc = attend_half(
-        half, q_t, da_t, far, far_exps, far_grads, near_total[...], near_acc[...]
+def far_kernel(half, sp_count, q, q_t, da, da_t, near_total, near_acc, *rest):
+    far, rest = rest[:sp_count], rest[sp_count:]
+    att_t, send, inv_totals, deltas, dq_acc, exps, prob_grads = rest
+    lanes, rows = q_t.shape[1], att_t.shape[1]
+    total, out_acc = attend(
+        half, q_t, da_t, far, exps, prob_grads, near_total[...], near_acc[...]
     )
     inv_total = 1.0 / total
     attended = (out_acc * inv_total).astype(BF16)
-    for h in range(heads):
+    for h in range(lanes // rows):
         att_t[h * HEAD : (h + 1) * HEAD, :] = attended[:, h * rows : (h + 1) * rows]
     delta = jnp.sum(attended.astype(F32) * da_t[...].astype(F32), axis=0, keepdims=True)
-    dq_acc = jnp.zeros((HEAD, lanes), F32)
-    for messages, exps, prob_grads, out in (
-        (far, far_exps, far_grads, send),
-        (near, near_exps, near_grads, keep),
-    ):
-        for k in range(sp_count):
-            span = slice(k * half, (k + 1) * half)
-            probs = exps[span, :] * inv_total
-            score_grad = (probs * (prob_grads[span, :] - delta)).astype(BF16)
-            at = 2 * k * half
-            dkey = nn(score_grad, q[...]) * inv_root
-            out[at : at + half, :] = dkey.astype(out.dtype)
-            dvalue = nn(probs.astype(BF16), da[...])
-            out[at + half : at + 2 * half, :] = dvalue.astype(out.dtype)
-            dq_acc = dq_acc + nn(messages[k][0:half, :].T, score_grad)
-    dq_t = (dq_acc * inv_root).astype(BF16)
-    for h in range(heads):
+    inv_totals[...] = inv_total
+    deltas[...] = delta
+    dq_acc[...] = pull_back(half, q, da, far, exps, prob_grads, inv_total, delta, send)
+
+
+def back_kernel(half, sp_count, q, da, exps, prob_grads, inv_totals, deltas, dq_acc, w_query, *rest):
+    near, (keep, t_keep, t_send, dq) = rest[:sp_count], rest[sp_count:]
+    rows = dq.shape[0]
+    acc = dq_acc[...] + pull_back(
+        half, q, da, near, exps, prob_grads, inv_totals[...], deltas[...], keep
+    )
+    dq_t = (acc * HEAD ** (-0.5)).astype(BF16)
+    for h in range(dq_t.shape[1] // rows):
         dq[:, h * HEAD : (h + 1) * HEAD] = dq_t[:, h * rows : (h + 1) * rows].T
-
-
-def pull_kernel(dq, w_query, keep, send):
-    half = keep.shape[0]
     pulled = nt(dq[...], w_query[...])
-    keep[...] = pulled[0:half]
-    send[...] = pulled[half:].astype(BF16)
+    t_keep[...] = pulled[0 : rows // 2]
+    t_send[...] = pulled[rows // 2 :].astype(BF16)
 
 
 def summed(refs, rows=slice(None)):
@@ -222,10 +237,12 @@
 def fold_core_kernel(keep, received, *refs):
     count = len(refs) // 2
     for k, (cot, message) in enumerate(zip(refs[:count], refs[count:])):
-        rows = message.shape[0] - cot.shape[0]
-        span = slice(k * rows, (k + 1) * rows)
-        message[0:rows, :] = summed((keep, received), span).astype(BF16)
-        message[rows:, :] = cot[...]
+        half = (message.shape[0] - cot.shape[0]) // 2
+        for part in range(2):
+            at = (part * count + k) * half
+            total = summed((keep, received), slice(at, at + half))
+            message[part * half : (part + 1) * half, :] = total.astype(BF16)
+        message[2 * half :, :] = cot[...]
 
 
 def fold_target_kernel(keep, received, *outs):
@@ -247,30 +264,42 @@
         cots[k * rows : (k + 1) * rows, :] = message[2 * half :, :]
 
 
+def prepare_kernel(rows, gain, w_key, w_value, unit, gained, inv, weights):
+    wide = rows[...].astype(F32)
+    inv_rms = inverse_rms(wide)
+    inv[...] = jnp.broadcast_to(inv_rms, inv.shape)
+    unit[...] = wide * inv_rms
+    gained[...] = wide * inv_rms * gain[...]
+    weights[0:HEAD, :] = w_key[...].T
+    weights[HEAD:, :] = w_value[...].T
+
+
 def finish_source_kernel(count, *refs):
-    parts, (rows, gain, w_key, w_value, out) = refs[:count], refs[count:]
+    parts, (unit, gained, inv, gain, weights, out) = refs[:count], refs[count:]
     grad = summed(parts).astype(BF16)
-    own = rows.shape[0]
-    pulled = nt(grad[0:own], w_key[...]) + nt(grad[own:], w_value[...])
-    out[...] = norm_back(rows[...], gain[...], pulled).astype(BF16)
+    own = unit.shape[0]
+    both = jnp.concatenate([grad[0:own], grad[own:]], axis=1)
+    pulled = nn(both, weights[...])
+    mean = jnp.mean(pulled * gained[...], axis=1, keepdims=True)
+    out[...] = (inv[:, 0:1] * (pulled * gain[...] - unit[...] * mean)).astype(BF16)
 
 
 def finish_target_kernel(count, z_count, *refs):
     parts, (part, gain), refs = refs[:z_count], refs[z_count : z_count + 2], refs[z_count + 2 :]
-    atts, (near, far, grad_target, grad_out, cots) = refs[:count], refs[count:]
+    atts, (near, far, grad_target, grad_out, cots, att_all) = refs[:count], refs[count:]
     grad_target[...] = norm_back(part[...], gain[...], summed(parts)).astype(BF16)
     pieces = grad_out.shape[1] // HEAD
-    rows = cots.shape[0] // 2
-    total = jnp.zeros(grad_out.shape, F32)
+    rows = cots.shape[0] // (2 * count)
     for k, att in enumerate(atts):
         first, second = (near, far) if k == 0 else (far, near)
         for piece in range(pieces):
             at = (k * pieces + piece) * rows
             column = slice(piece * HEAD, (piece + 1) * HEAD)
-            cots[0:rows, column] = first[at : at + rows, :]
-            cots[rows:, column] = second[at : at + rows, :]
-        total = total + nn(att[...], cots[...])
-    grad_out[...] = total.astype(BF16)
+            top = 2 * k * rows
+            cots[top : top + rows, column] = first[at : at + rows, :]
+            cots[top + rows : top + 2 * rows, column] = second[at : at + rows, :]
+        att_all[:, 2 * k * rows : 2 * (k + 1) * rows] = att[...]
+    grad_out[...] = nn(att_all[...], cots[...]).astype(BF16)
 
 
 def on_device(target, source, cotangent, target_gain, source_gain, w_query, w_key, w_value, w_out):
@@ -339,31 +368,45 @@
         + [pltpu.SemaphoreType.DMA((n,)) for n in (t_blocks, t_blocks, 2)],
     )(in_hbm(target), in_hbm(cotangent), in_hbm(target_gain), w_query, in_hbm(w_out))
 
+    unit, gained, inv, weights = call(
+        prepare_kernel,
+        [shape((s_own, width), F32)] * 2
+        + [shape((s_own, HEAD), F32), shape((2 * HEAD, width), BF16)],
+        8 * s_own * width, 8 * width * HEAD, [VMEM] * 4, (),
+    )(source_part, source_gain, w_key, w_value)
+    prepared = (unit, gained, inv, source_gain, weights)
+
     stats = call(
         functools.partial(near_kernel, s_half, sp_count),
         [shape((far_rows, lanes), F32)] * 2 + [shape((1, lanes), F32), shape((HEAD, lanes), F32)],
         6 * lanes * far_rows * HEAD, 8 * far_rows * lanes,
         [VMEM] * (2 + sp_count), (),
     )(q_t, da_t, *near)
-    att_t, dq, keep, send = call(
+    exps, prob_grads, total, out_acc = stats
+    att_t, send, inv_total, delta, dq_acc = call(
         functools.partial(far_kernel, s_half, sp_count),
         [
             shape((q_width, t_rows), BF16),
-            shape((t_rows, q_width), BF16),
+            shape((2 * far_rows, HEAD), BF16),
+            shape((1, lanes), F32),
+            shape((1, lanes), F32),
+            shape((HEAD, lanes), F32),
+        ],
+        12 * lanes * far_rows * HEAD, 8 * far_rows * lanes,
+        [VMEM] * (6 + sp_count), [pltpu.VMEM((far_rows, lanes), F32)] * 2,
+    )(q, q_t, da, da_t, total, out_acc, *far)
+    received = to_core(send)
+    keep, t_keep, t_send = call(
+        functools.partial(back_kernel, s_half, sp_count),
+        [
             shape((2 * far_rows, HEAD), F32),
-            shape((2 * far_rows, HEAD), BF16),
+            shape((t_half, width), F32),
+            shape((t_half, width), BF16),
         ],
-        18 * lanes * far_rows * HEAD, 8 * far_rows * lanes,
-        [VMEM] * (8 + 2 * sp_count), [pltpu.VMEM((far_rows, lanes), F32)] * 2,
-    )(q, q_t, da, da_t, *stats, *near, *far)
-
-    received = to_core(send)
-    t_keep, t_send = call(
-        pull_kernel,
-        [shape((t_half, width), F32), shape((t_half, width), BF16)],
-        2 * t_rows * width * q_width, 2 * width * q_width + 8 * t_rows * width,
-        [VMEM, VMEM], (),
-    )(dq, w_query)
+        6 * lanes * far_rows * HEAD + 2 * t_rows * width * q_width,
+        8 * far_rows * lanes + 2 * width * q_width,
+        [VMEM] * (8 + sp_count), [pltpu.VMEM((t_rows, q_width), BF16)],
+    )(q, da, exps, prob_grads, inv_total, delta, dq_acc, w_query, *near)
     t_received = to_core(t_send)
     messages = call(
         fold_core_kernel, [shape((2 * s_half + cot_rows, HEAD), BF16)] * sp_count,
@@ -398,12 +441,15 @@
         functools.partial(finish_target_kernel, sp_count, z_count),
         [shape((t_own, width), BF16), shape((q_width, width // sp_count), BF16)],
         2 * q_width * width * t_rows, 2 * q_width * width, [VMEM] * (z_count + sp_count + 4),
-        [pltpu.VMEM((t_rows, width // sp_count), BF16)],
+        [
+            pltpu.VMEM((sp_count * t_rows, width // sp_count), BF16),
+            pltpu.VMEM((q_width, sp_count * t_rows), BF16),
+        ],
     )(*t_parts, target_part, target_gain, *atts, cots, far_cots)
     grad_source = call(
         functools.partial(finish_source_kernel, z_count), shape((s_own, width), BF16),
-        4 * s_own * width * HEAD, 4 * width * HEAD, [VMEM] * (z_count + 4), (),
-    )(*s_parts, source_part, source_gain, w_key, w_value)
+        4 * s_own * width * HEAD, 4 * width * HEAD, [VMEM] * (z_count + 5), (),
+    )(*s_parts, *prepared)
     return (grad_target, grad_source, grad_out)
 
 

time: 56.9 us -> 55.4 us (0.974)
  the two profiles are of different devices: /device:TPU:0 before, /device:TPU:1 now
where the time goes in v2:
time: 55.4 us; the launch traced here: 55.2 us
  starting transfers between devices  24.6 us (44%)
  waiting for transfers between devices  17.3 us (31%)
  Pallas kernels  12.6 us (23%)
  between operations  0.78 us (1%)
    ppermute x22, starting transfers between devices, swap(): return lax.ppermute(value, ('sp', 'tp'), pairs)  24.6 us
    ppermute x22, waiting for transfers between devices, swap(): return lax.ppermute(value, ('sp', 'tp'), pairs)  17.3 us
    pallas_call x1, Pallas kernels, on_device(): call(functools.partial(target_kernel, t_blocks, t_own, sp_count), [shape(...  3.13 us
    pallas_call x1, Pallas kernels, on_device(): call(functools.partial(source_kernel, s_blocks, s_own), [shape((2 * s_hal...  2.1 us
    pallas_call x1, Pallas kernels, on_device(): call(functools.partial(far_kernel, s_half, sp_count), [shape((q_width, t_...  1.92 us
    pallas_call x1, Pallas kernels, on_device(): call(functools.partial(back_kernel, s_half, sp_count), [shape((2 * far_ro...  1.53 us
    pallas_call x1, Pallas kernels, on_device(): call(functools.partial(finish_target_kernel, sp_count, z_count), [shape((...  1.36 us
  transfers between devices with their start and end apart: 22, of which 9 were waited for; matrix products, arithmetic and copies ran while one was open for 0% of the time, Pallas kernels for 13%

profile of v2, /device:TPU:1, one launch (start us, length us, event | category | flops | bytes accessed | tf_op | source)
XLA Modules:
  0.0 55.2 jit_solution(6423354161863738670)
XLA Ops:
  0.6 2.1 %shard_map.113 = (bf16[384,128]{1,0:T(8,128)(2,1)S(1)}, bf16[48,2048]{1,0:T(8,128)(2,1)S(1)}) custom-call(bf16[384,2048]{1,0:T(8,128)(2,1)} %source.1, f32[1,2048]{1,0:T(1,128)} %bitcast.2, bf16[2048,128]{1,0:T(8,128)(2,1)} %w_key.3, bf16[2048,128]{1,0:T(8,128)(2,1)} %w_value.3), custom_call_target="tpu_custom_call" | custom-call | flops 201326592 | bytes 2621440 | tf_op jit(solution)/shard_map/pallas_call | solution.py:343
  2.7 2.7 %collective-permute-start = (bf16[384,128]{1,0:T(8,128)(2,1)S(1)}, bf16[384,128]{1,0:T(8,128)(2,1)S(1)}, u32[]{:S(2)}, u32[]{:S(2)}) collective-permute-start(bf16[384,128]{1,0:T(8,128)(2,1)S(1)} %get-tuple-element.49.rest_0_), channel_id=1, source_target_pairs={{0,9},{1,8},{2,11},{3,10},{4,13},{5,12},{6,15},{7,14},{8,1},{9,0},... | collective-permute-start | bytes 294920 | tf_op jit(solution)/shard_map/ppermute | solution.py:322
  5.4 1.0 %collective-permute-start.1 = (bf16[384,128]{1,0:T(8,128)(2,1)S(1)}, bf16[384,128]{1,0:T(8,128)(2,1)S(1)}, u32[]{:S(2)}, u32[]{:S(2)}) collective-permute-start(bf16[384,128]{1,0:T(8,128)(2,1)S(1)} %get-tuple-element.49.rest_0_), channel_id=1, source_target_pairs={{0,17},{1,16},{2,19},{3,18},{4,21},{5,20},{6,23},{7,22},{8,25},{9,... | collective-permute-start | bytes 294920 | tf_op jit(solution)/shard_map/ppermute | solution.py:322
  6.4 0.2 collective-permute-start.2
  6.5 0.5 collective-permute-start.3
  7.1 1.1 %collective-permute-done.rest_1_ = bf16[384,128]{1,0:T(8,128)(2,1)S(1)} collective-permute-done((bf16[384,128]{1,0:T(8,128)(2,1)S(1)}, bf16[384,128]{1,0:T(8,128)(2,1)S(1)}, u32[]{:S(2)}, u32[]{:S(2)}) %collective-permute-start) | collective-permute-done | bytes 98336 | tf_op jit(solution)/shard_map/ppermute | solution.py:322
  8.2 0.2 collective-permute-start.4
  8.4 1.3 %collective-permute-done.1.rest_2_ = bf16[384,128]{1,0:T(8,128)(2,1)S(1)} collective-permute-done((bf16[384,128]{1,0:T(8,128)(2,1)S(1)}, bf16[384,128]{1,0:T(8,128)(2,1)S(1)}, u32[]{:S(2)}, u32[]{:S(2)}) %collective-permute-start.1) | collective-permute-done | bytes 98336 | tf_op jit(solution)/shard_map/ppermute | solution.py:322
  9.7 1.8 %collective-permute-start.5 = (bf16[384,128]{1,0:T(8,128)(2,1)S(1)}, bf16[384,128]{1,0:T(8,128)(2,1)S(1)}, u32[]{:S(2)}, u32[]{:S(2)}) collective-permute-start(bf16[384,128]{1,0:T(8,128)(2,1)S(1)} %collective-permute-done.1.rest_2_), channel_id=1, source_target_pairs={{0,1},{1,0},{2,3},{3,2},{4,5},{5,4},{6,7},{7,6},{8,9},{9,8},{10,11... | collective-permute-start | bytes 294920 | tf_op jit(solution)/shard_map/ppermute | solution.py:322
  11.5 1.1 %collective-permute-done.2.rest_3_ = bf16[384,128]{1,0:T(8,128)(2,1)S(1)} collective-permute-done((bf16[384,128]{1,0:T(8,128)(2,1)S(1)}, bf16[384,128]{1,0:T(8,128)(2,1)S(1)}, u32[]{:S(2)}, u32[]{:S(2)}) %collective-permute-start.2) | collective-permute-done | bytes 98336 | tf_op jit(solution)/shard_map/ppermute | solution.py:322
  12.6 0.4 collective-permute-start.6
  13.0 3.1 %shard_map.112 = (bf16[512,128]{1,0:T(8,128)(2,1)S(1)}, bf16[128,512]{1,0:T(8,128)(2,1)S(1)}, bf16[512,128]{1,0:T(8,128)(2,1)S(1)}, bf16[128,512]{1,0:T(8,128)(2...) custom-call(bf16[128,2048]{1,0:T(8,128)(2,1)} %target.1, ...), custom_call_target="tpu_custom_call" | custom-call | flops 536870912 | bytes 5242880 | tf_op jit(solution)/shard_map/pallas_call | solution.py:359
  16.2 0.8 %shard_map.114 = (f32[768,512]{1,0:T(8,128)S(1)}, f32[768,512]{1,0:T(8,128)S(1)}, f32[1,512]{1,0:T(1,128)S(1)}, f32[128,512]{1,0:T(8,128)S(1)}) custom-call(bf16[128,512]{1,0:T(8,128)(2,1)S(1)} %get-tuple-element.47.q_t, bf16[128,512]{1,0:T(8,128)(2,1)S(1)} %get-tuple-element.48.da_t, bf16[384,128]{1,0:T(8,128)(2,1)S(1)} %get-tuple-element.49.rest_0_, ...), custom_call_target="tpu_custom_call" | custom-call | flops 301989888 | bytes 3145728 | tf_op jit(solution)/shard_map/pallas_call | solution.py:379
  17.0 0.0 collective-permute-done.4.rest_1_
  17.0 0.0 collective-permute-done.5.rest_2_
  17.0 1.9 %shard_map.115 = (bf16[512,128]{1,0:T(8,128)(2,1)S(1)}, bf16[1536,128]{1,0:T(8,128)(2,1)S(1)}, f32[1,512]{1,0:T(1,128)S(1)}, f32[1,512]{1,0:T(1,128)S(1)}, f32[128,512]{1,0:T(8,128)S(1)}) custom-call(bf16[512,128]{1,0:T(8,128)(2,1)S(1)} %get-tuple-element.45.q, bf16[128,512]{1,0:T(8,128)(2,1)S(1)} %get-tuple-element.47.q_t, ...), custom_call_target="tpu_custom_call" | custom-call | flops 603979776 | bytes 3145728 | tf_op jit(solution)/shard_map/pallas_call | solution.py:386
  18.9 0.2 collective-permute-start.14
  19.1 1.5 %shard_map.116 = (f32[1536,128]{1,0:T(8,128)S(1)}, f32[64,2048]{1,0:T(8,128)S(1)}, bf16[64,2048]{1,0:T(8,128)(2,1)S(1)}) custom-call(bf16[512,128]{1,0:T(8,128)(2,1)S(1)} %get-tuple-element.45.q, bf16[512,128]{1,0:T(8,128)(2,1)S(1)} %get-tuple-element.46.da, f32[768,512]{1,0:T(8,128)S(1)} %get-tuple-element.50.exps, ...), custom_call_target="tpu_custom_call" | custom-call | flops 570425344 | bytes 5242880 | tf_op jit(solution)/shard_map/pallas_call | solution.py:399
  20.7 0.0 copy-start.1
  20.7 0.0 copy-start.2
  20.7 0.0 copy-start.3
  20.7 0.0 collective-permute-done.14.received
  20.7 0.1 shard_map.118
  20.8 1.0 %collective-permute-start.15 = (bf16[640,128]{1,0:T(8,128)(2,1)S(1)}, bf16[640,128]{1,0:T(8,128)(2,1)S(1)}, u32[]{:S(2)}, u32[]{:S(2)}) collective-permute-start(bf16[640,128]{1,0:T(8,128)(2,1)S(1)} %get-tuple-element.72), channel_id=1, source_target_pairs={{0,9},{1,8},{2,11},{3,10},{4,13},{5,12},{6,15},{7,14},{8,1},{9,0},... | collective-permute-start | bytes 491528 | tf_op jit(solution)/shard_map/ppermute | solution.py:322
  21.8 0.4 collective-permute-start.16
  22.2 1.9 %collective-permute-start.17 = (bf16[640,128]{1,0:T(8,128)(2,1)S(1)}, bf16[640,128]{1,0:T(8,128)(2,1)S(1)}, u32[]{:S(2)}, u32[]{:S(2)}) collective-permute-start(bf16[640,128]{1,0:T(8,128)(2,1)S(1)} %get-tuple-element.74), channel_id=1, source_target_pairs={{0,25},{1,24},{2,27},{3,26},{4,29},{5,28},{6,31},{7,30},{8,17},{9,... | collective-permute-start | bytes 491528 | tf_op jit(solution)/shard_map/ppermute | solution.py:322
  24.1 0.1 collective-permute-start.7
  24.2 3.5 %collective-permute-done.15.refs_1_ = bf16[640,128]{1,0:T(8,128)(2,1)S(1)} collective-permute-done((bf16[640,128]{1,0:T(8,128)(2,1)S(1)}, bf16[640,128]{1,0:T(8,128)(2,1)S(1)}, u32[]{:S(2)}, u32[]{:S(2)}) %collective-permute-start.15) | collective-permute-done | bytes 163872 | tf_op jit(solution)/shard_map/ppermute | solution.py:322
  27.7 3.6 %collective-permute-done.16.refs_2_ = bf16[640,128]{1,0:T(8,128)(2,1)S(1)} collective-permute-done((bf16[640,128]{1,0:T(8,128)(2,1)S(1)}, bf16[640,128]{1,0:T(8,128)(2,1)S(1)}, u32[]{:S(2)}, u32[]{:S(2)}) %collective-permute-start.16) | collective-permute-done | bytes 163872 | tf_op jit(solution)/shard_map/ppermute | solution.py:322
  31.3 0.1 shard_map.119
  31.3 0.1 collective-permute-start.18
  31.4 0.9 %collective-permute-start.11 = (bf16[512,128]{1,0:T(8,128)(2,1)S(1)}, bf16[512,128]{1,0:T(8,128)(2,1)S(1)}, u32[]{:S(2)}, u32[]{:S(2)}) collective-permute-start(bf16[512,128]{1,0:T(8,128)(2,1)S(1)} %get-tuple-element.64.refs_6_), channel_id=1, source_target_pairs={{0,8},{1,9},{2,10},{3,11},{4,12},{5,13},{6,14},{7,15},{8,0},{9,1},... | collective-permute-start | bytes 393224 | tf_op jit(solution)/shard_map/ppermute | solution.py:322
  32.3 0.7 %collective-permute-start.12 = (bf16[512,128]{1,0:T(8,128)(2,1)S(1)}, bf16[512,128]{1,0:T(8,128)(2,1)S(1)}, u32[]{:S(2)}, u32[]{:S(2)}) collective-permute-start(bf16[512,128]{1,0:T(8,128)(2,1)S(1)} %get-tuple-element.64.refs_6_), channel_id=1, source_target_pairs={{0,16},{1,17},{2,18},{3,19},{4,20},{5,21},{6,22},{7,23},{8,24},{9,... | collective-permute-start | bytes 393224 | tf_op jit(solution)/shard_map/ppermute | solution.py:322
  33.0 1.1 %collective-permute-start.13 = (bf16[512,128]{1,0:T(8,128)(2,1)S(1)}, bf16[512,128]{1,0:T(8,128)(2,1)S(1)}, u32[]{:S(2)}, u32[]{:S(2)}) collective-permute-start(bf16[512,128]{1,0:T(8,128)(2,1)S(1)} %get-tuple-element.64.refs_6_), channel_id=1, source_target_pairs={{0,24},{1,25},{2,26},{3,27},{4,28},{5,29},{6,30},{7,31},{8,16},{9,... | collective-permute-start | bytes 393224 | tf_op jit(solution)/shard_map/ppermute | solution.py:322
  34.1 2.0 %collective-permute-done.11.refs_7_ = bf16[512,128]{1,0:T(8,128)(2,1)S(1)} collective-permute-done((bf16[512,128]{1,0:T(8,128)(2,1)S(1)}, bf16[512,128]{1,0:T(8,128)(2,1)S(1)}, u32[]{:S(2)}, u32[]{:S(2)}) %collective-permute-start.11) | collective-permute-done | bytes 131104 | tf_op jit(solution)/shard_map/ppermute | solution.py:322
  36.1 3.2 %collective-permute-start.19 = (bf16[96,128]{1,0:T(8,128)(2,1)S(1)}, bf16[96,128]{1,0:T(8,128)(2,1)S(1)}, u32[]{:S(2)}, u32[]{:S(2)}) collective-permute-start(bf16[96,128]{1,0:T(8,128)(2,1)S(1)} %get-tuple-element.78), channel_id=1, source_target_pairs={{0,3},{1,2},{2,1},{3,0},{4,7},{5,6},{6,5},{7,4},{8,11},{9,10},{10,... | collective-permute-start | bytes 73736 | tf_op jit(solution)/shard_map/ppermute | solution.py:322
  39.3 4.0 %collective-permute-start.20 = (bf16[96,128]{1,0:T(8,128)(2,1)S(1)}, bf16[96,128]{1,0:T(8,128)(2,1)S(1)}, u32[]{:S(2)}, u32[]{:S(2)}) collective-permute-start(bf16[96,128]{1,0:T(8,128)(2,1)S(1)} %get-tuple-element.79), channel_id=1, source_target_pairs={{0,5},{1,4},{2,7},{3,6},{4,1},{5,0},{6,3},{7,2},{8,13},{9,12},{10,... | collective-permute-start | bytes 73736 | tf_op jit(solution)/shard_map/ppermute | solution.py:322
  43.3 1.0 %collective-permute-start.21 = (bf16[96,128]{1,0:T(8,128)(2,1)S(1)}, bf16[96,128]{1,0:T(8,128)(2,1)S(1)}, u32[]{:S(2)}, u32[]{:S(2)}) collective-permute-start(bf16[96,128]{1,0:T(8,128)(2,1)S(1)} %get-tuple-element.80), channel_id=1, source_target_pairs={{0,7},{1,6},{2,5},{3,4},{4,3},{5,2},{6,1},{7,0},{8,15},{9,14},{10,... | collective-permute-start | bytes 73736 | tf_op jit(solution)/shard_map/ppermute | solution.py:322
  44.3 0.1 shard_map.117
  44.4 2.6 %collective-permute-start.10 = (bf16[16,2048]{1,0:T(8,128)(2,1)S(1)}, bf16[16,2048]{1,0:T(8,128)(2,1)S(1)}, u32[]{:S(2)}, u32[]{:S(2)}) collective-permute-start(bf16[16,2048]{1,0:T(8,128)(2,1)S(1)} %get-tuple-element.62), channel_id=1, source_target_pairs={{0,7},{1,6},{2,5},{3,4},{4,3},{5,2},{6,1},{7,0},{8,15},{9,14},{10,... | collective-permute-start | bytes 196616 | tf_op jit(solution)/shard_map/ppermute | solution.py:322
  47.0 1.5 %collective-permute-done.21.refs_3_ = bf16[96,128]{1,0:T(8,128)(2,1)S(1)} collective-permute-done((bf16[96,128]{1,0:T(8,128)(2,1)S(1)}, bf16[96,128]{1,0:T(8,128)(2,1)S(1)}, u32[]{:S(2)}, u32[]{:S(2)}) %collective-permute-start.21) | collective-permute-done | bytes 24608 | tf_op jit(solution)/shard_map/ppermute | solution.py:322
  48.4 0.7 %collective-permute-start.9 = (bf16[16,2048]{1,0:T(8,128)(2,1)S(1)}, bf16[16,2048]{1,0:T(8,128)(2,1)S(1)}, u32[]{:S(2)}, u32[]{:S(2)}) collective-permute-start(bf16[16,2048]{1,0:T(8,128)(2,1)S(1)} %get-tuple-element.61), channel_id=1, source_target_pairs={{0,5},{1,4},{2,7},{3,6},{4,1},{5,0},{6,3},{7,2},{8,13},{9,12},{10,... | collective-permute-start | bytes 196616 | tf_op jit(solution)/shard_map/ppermute | solution.py:322
  49.1 0.4 shard_map.121
  49.5 1.1 %shard_map.122 = bf16[48,2048]{1,0:T(8,128)(2,1)} custom-call(bf16[96,128]{1,0:T(8,128)(2,1)S(1)} %get-tuple-element.77.refs_0_, bf16[96,128]{1,0:T(8,128)(2,1)S(1)} %collective-permute-done.19.refs_1_, bf16[96,128]{1,0:T(8,128)(2,1)S(1)} %collective-permute-done.20.refs_2_, bf16[96,128]{1,0:T(8,128)(2,1)S(1)} %collective-permute-done.21.refs_3_, ...), custom_call_target="tpu_custom_call" | custom-call | flops 50331648 | bytes 1048576 | tf_op jit(solution)/shard_map/pallas_call | solution.py:449
  50.6 0.0 collective-permute-done.10.refs_3_
  50.6 1.2 %collective-permute-done.8.refs_1_ = bf16[16,2048]{1,0:T(8,128)(2,1)S(1)} collective-permute-done((bf16[16,2048]{1,0:T(8,128)(2,1)S(1)}, bf16[16,2048]{1,0:T(8,128)(2,1)S(1)}, u32[]{:S(2)}, u32[]{:S(2)}) %collective-permute-start.8) | collective-permute-done | bytes 65568 | tf_op jit(solution)/shard_map/ppermute | solution.py:322
  51.8 2.1 %collective-permute-done.9.refs_2_ = bf16[16,2048]{1,0:T(8,128)(2,1)S(1)} collective-permute-done((bf16[16,2048]{1,0:T(8,128)(2,1)S(1)}, bf16[16,2048]{1,0:T(8,128)(2,1)S(1)}, u32[]{:S(2)}, u32[]{:S(2)}) %collective-permute-start.9) | collective-permute-done | bytes 65568 | tf_op jit(solution)/shard_map/ppermute | solution.py:322
  53.9 1.4 %shard_map.120 = (bf16[16,2048]{1,0:T(8,128)(2,1)}, bf16[512,512]{1,0:T(8,128)(2,1)}) custom-call(bf16[16,2048]{1,0:T(8,128)(2,1)S(1)} %get-tuple-element.59.refs_0_, bf16[16,2048]{1,0:T(8,128)(2,1)S(1)} %collective-permute-done.8.refs_1_, bf16[16,2048]{1,0:T(8,128)(2,1)S(1)} %collective-permute-done.9.refs_2_, ...), custom_call_target="tpu_custom_call" | custom-call | flops 268435456 | bytes 2097152 | tf_op jit(solution)/shard_map/pallas_call | solution.py:440
  (17 shorter events, 0.0 us)
Async XLA Ops:
  0.6 12.4 %copy-start = (bf16[2048,512]{1,0:T(8,128)(2,1)S(1)}, bf16[2048,512]{1,0:T(8,128)(2,1)}, u32[]{:S(2)}) copy-start(bf16[2048,512]{1,0:T(8,128)(2,1)} %w_query.3) | copy-start | bytes 6291460
  2.7 5.4 %collective-permute-start = (bf16[384,128]{1,0:T(8,128)(2,1)S(1)}, bf16[384,128]{1,0:T(8,128)(2,1)S(1)}, u32[]{:S(2)}, u32[]{:S(2)}) collective-permute-start(bf16[384,128]{1,0:T(8,128)(2,1)S(1)} %get-tuple-element.49.rest_0_), channel_id=1, source_target_pairs={{0,9},{1,8},{2,11},{3,10},{4,13},{5,12},{6,15},{7,14},{8,1},{9,0},... | collective-permute-start | bytes 294920 | tf_op jit(solution)/shard_map/ppermute | solution.py:322
  5.4 4.3 %collective-permute-start.1 = (bf16[384,128]{1,0:T(8,128)(2,1)S(1)}, bf16[384,128]{1,0:T(8,128)(2,1)S(1)}, u32[]{:S(2)}, u32[]{:S(2)}) collective-permute-start(bf16[384,128]{1,0:T(8,128)(2,1)S(1)} %get-tuple-element.49.rest_0_), channel_id=1, source_target_pairs={{0,17},{1,16},{2,19},{3,18},{4,21},{5,20},{6,23},{7,22},{8,25},{9,... | collective-permute-start | bytes 294920 | tf_op jit(solution)/shard_map/ppermute | solution.py:322
  6.4 6.3 %collective-permute-start.2 = (bf16[384,128]{1,0:T(8,128)(2,1)S(1)}, bf16[384,128]{1,0:T(8,128)(2,1)S(1)}, u32[]{:S(2)}, u32[]{:S(2)}) collective-permute-start(bf16[384,128]{1,0:T(8,128)(2,1)S(1)} %get-tuple-element.49.rest_0_), channel_id=1, source_target_pairs={{0,25},{1,24},{2,27},{3,26},{4,29},{5,28},{6,31},{7,30},{8,17},{9,... | collective-permute-start | bytes 294920 | tf_op jit(solution)/shard_map/ppermute | solution.py:322
  6.5 10.5 %collective-permute-start.3 = (bf16[384,128]{1,0:T(8,128)(2,1)S(1)}, bf16[384,128]{1,0:T(8,128)(2,1)S(1)}, u32[]{:S(2)}, u32[]{:S(2)}) collective-permute-start(bf16[384,128]{1,0:T(8,128)(2,1)S(1)} %get-tuple-element.49.rest_0_), channel_id=1, source_target_pairs={{0,1},{1,0},{2,3},{3,2},{4,5},{5,4},{6,7},{7,6},{8,9},{9,8},{10,11... | collective-permute-start | bytes 294920 | tf_op jit(solution)/shard_map/ppermute | solution.py:322
  8.2 8.8 %collective-permute-start.4 = (bf16[384,128]{1,0:T(8,128)(2,1)S(1)}, bf16[384,128]{1,0:T(8,128)(2,1)S(1)}, u32[]{:S(2)}, u32[]{:S(2)}) collective-permute-start(bf16[384,128]{1,0:T(8,128)(2,1)S(1)} %collective-permute-done.rest_1_), channel_id=1, source_target_pairs={{0,1},{1,0},{2,3},{3,2},{4,5},{5,4},{6,7},{7,6},{8,9},{9,8},{10,11... | collective-permute-start | bytes 294920 | tf_op jit(solution)/shard_map/ppermute | solution.py:322
  9.7 7.3 %collective-permute-start.5 = (bf16[384,128]{1,0:T(8,128)(2,1)S(1)}, bf16[384,128]{1,0:T(8,128)(2,1)S(1)}, u32[]{:S(2)}, u32[]{:S(2)}) collective-permute-start(bf16[384,128]{1,0:T(8,128)(2,1)S(1)} %collective-permute-done.1.rest_2_), channel_id=1, source_target_pairs={{0,1},{1,0},{2,3},{3,2},{4,5},{5,4},{6,7},{7,6},{8,9},{9,8},{10,11... | collective-permute-start | bytes 294920 | tf_op jit(solution)/shard_map/ppermute | solution.py:322
  12.6 4.4 %collective-permute-start.6 = (bf16[384,128]{1,0:T(8,128)(2,1)S(1)}, bf16[384,128]{1,0:T(8,128)(2,1)S(1)}, u32[]{:S(2)}, u32[]{:S(2)}) collective-permute-start(bf16[384,128]{1,0:T(8,128)(2,1)S(1)} %collective-permute-done.2.rest_3_), channel_id=1, source_target_pairs={{0,1},{1,0},{2,3},{3,2},{4,5},{5,4},{6,7},{7,6},{8,9},{9,8},{10,11... | collective-permute-start | bytes 294920 | tf_op jit(solution)/shard_map/ppermute | solution.py:322
  18.9 1.8 %collective-permute-start.14 = (bf16[1536,128]{1,0:T(8,128)(2,1)S(1)}, bf16[1536,128]{1,0:T(8,128)(2,1)S(1)}, u32[]{:S(2)}, u32[]{:S(2)}) collective-permute-start(bf16[1536,128]{1,0:T(8,128)(2,1)S(1)} %get-tuple-element.66), channel_id=1, source_target_pairs={{0,1},{1,0},{2,3},{3,2},{4,5},{5,4},{6,7},{7,6},{8,9},{9,8},{10,11... | collective-permute-start | bytes 1179656 | tf_op jit(solution)/shard_map/ppermute | solution.py:322
  20.7 28.4 %copy-start.1 = (bf16[2048,128]{1,0:T(8,128)(2,1)S(1)}, bf16[2048,128]{1,0:T(8,128)(2,1)}, u32[]{:S(2)}) copy-start(bf16[2048,128]{1,0:T(8,128)(2,1)} %w_key.3) | copy-start | bytes 1572868
  20.7 28.4 %copy-start.2 = (bf16[2048,128]{1,0:T(8,128)(2,1)S(1)}, bf16[2048,128]{1,0:T(8,128)(2,1)}, u32[]{:S(2)}) copy-start(bf16[2048,128]{1,0:T(8,128)(2,1)} %w_value.3) | copy-start | bytes 1572868
  20.7 28.4 %copy-start.3 = (f32[2048]{0:T(1024)S(1)}, f32[2048]{0:T(1024)}, u32[]{:S(2)}) copy-start(f32[2048]{0:T(1024)} %param.13) | copy-start | bytes 24580
  20.8 6.9 %collective-permute-start.15 = (bf16[640,128]{1,0:T(8,128)(2,1)S(1)}, bf16[640,128]{1,0:T(8,128)(2,1)S(1)}, u32[]{:S(2)}, u32[]{:S(2)}) collective-permute-start(bf16[640,128]{1,0:T(8,128)(2,1)S(1)} %get-tuple-element.72), channel_id=1, source_target_pairs={{0,9},{1,8},{2,11},{3,10},{4,13},{5,12},{6,15},{7,14},{8,1},{9,0},... | collective-permute-start | bytes 491528 | tf_op jit(solution)/shard_map/ppermute | solution.py:322
  21.8 9.5 %collective-permute-start.16 = (bf16[640,128]{1,0:T(8,128)(2,1)S(1)}, bf16[640,128]{1,0:T(8,128)(2,1)S(1)}, u32[]{:S(2)}, u32[]{:S(2)}) collective-permute-start(bf16[640,128]{1,0:T(8,128)(2,1)S(1)} %get-tuple-element.73), channel_id=1, source_target_pairs={{0,17},{1,16},{2,19},{3,18},{4,21},{5,20},{6,23},{7,22},{8,25},{9,... | collective-permute-start | bytes 491528 | tf_op jit(solution)/shard_map/ppermute | solution.py:322
  22.2 9.0 %collective-permute-start.17 = (bf16[640,128]{1,0:T(8,128)(2,1)S(1)}, bf16[640,128]{1,0:T(8,128)(2,1)S(1)}, u32[]{:S(2)}, u32[]{:S(2)}) collective-permute-start(bf16[640,128]{1,0:T(8,128)(2,1)S(1)} %get-tuple-element.74), channel_id=1, source_target_pairs={{0,25},{1,24},{2,27},{3,26},{4,29},{5,28},{6,31},{7,30},{8,17},{9,... | collective-permute-start | bytes 491528 | tf_op jit(solution)/shard_map/ppermute | solution.py:322
  24.1 19.2 %collective-permute-start.7 = (bf16[64,2048]{1,0:T(8,128)(2,1)S(1)}, bf16[64,2048]{1,0:T(8,128)(2,1)S(1)}, u32[]{:S(2)}, u32[]{:S(2)}) collective-permute-start(bf16[64,2048]{1,0:T(8,128)(2,1)S(1)} %get-tuple-element.58), channel_id=1, source_target_pairs={{0,1},{1,0},{2,3},{3,2},{4,5},{5,4},{6,7},{7,6},{8,9},{9,8},{10,11... | collective-permute-start | bytes 786440 | tf_op jit(solution)/shard_map/ppermute | solution.py:322
  31.3 22.6 %collective-permute-start.18 = (bf16[1024,128]{1,0:T(8,128)(2,1)S(1)}, bf16[1024,128]{1,0:T(8,128)(2,1)S(1)}, u32[]{:S(2)}, u32[]{:S(2)}) collective-permute-start(bf16[1024,128]{1,0:T(8,128)(2,1)S(1)} %get-tuple-element.75.refs_10_), channel_id=1, source_target_pairs={{0,1},{1,0},{2,3},{3,2},{4,5},{5,4},{6,7},{7,6},{8,9},{9,8},{10,11... | collective-permute-start | bytes 786440 | tf_op jit(solution)/shard_map/ppermute | solution.py:322
  31.4 4.7 %collective-permute-start.11 = (bf16[512,128]{1,0:T(8,128)(2,1)S(1)}, bf16[512,128]{1,0:T(8,128)(2,1)S(1)}, u32[]{:S(2)}, u32[]{:S(2)}) collective-permute-start(bf16[512,128]{1,0:T(8,128)(2,1)S(1)} %get-tuple-element.64.refs_6_), channel_id=1, source_target_pairs={{0,8},{1,9},{2,10},{3,11},{4,12},{5,13},{6,14},{7,15},{8,0},{9,1},... | collective-permute-start | bytes 393224 | tf_op jit(solution)/shard_map/ppermute | solution.py:322
  32.3 7.0 %collective-permute-start.12 = (bf16[512,128]{1,0:T(8,128)(2,1)S(1)}, bf16[512,128]{1,0:T(8,128)(2,1)S(1)}, u32[]{:S(2)}, u32[]{:S(2)}) collective-permute-start(bf16[512,128]{1,0:T(8,128)(2,1)S(1)} %get-tuple-element.64.refs_6_), channel_id=1, source_target_pairs={{0,16},{1,17},{2,18},{3,19},{4,20},{5,21},{6,22},{7,23},{8,24},{9,... | collective-permute-start | bytes 393224 | tf_op jit(solution)/shard_map/ppermute | solution.py:322
  33.0 17.6 %collective-permute-start.13 = (bf16[512,128]{1,0:T(8,128)(2,1)S(1)}, bf16[512,128]{1,0:T(8,128)(2,1)S(1)}, u32[]{:S(2)}, u32[]{:S(2)}) collective-permute-start(bf16[512,128]{1,0:T(8,128)(2,1)S(1)} %get-tuple-element.64.refs_6_), channel_id=1, source_target_pairs={{0,24},{1,25},{2,26},{3,27},{4,28},{5,29},{6,30},{7,31},{8,16},{9,... | collective-permute-start | bytes 393224 | tf_op jit(solution)/shard_map/ppermute | solution.py:322
  36.1 8.3 %collective-permute-start.19 = (bf16[96,128]{1,0:T(8,128)(2,1)S(1)}, bf16[96,128]{1,0:T(8,128)(2,1)S(1)}, u32[]{:S(2)}, u32[]{:S(2)}) collective-permute-start(bf16[96,128]{1,0:T(8,128)(2,1)S(1)} %get-tuple-element.78), channel_id=1, source_target_pairs={{0,3},{1,2},{2,1},{3,0},{4,7},{5,6},{6,5},{7,4},{8,11},{9,10},{10,... | collective-permute-start | bytes 73736 | tf_op jit(solution)/shard_map/ppermute | solution.py:322
  39.3 7.7 %collective-permute-start.20 = (bf16[96,128]{1,0:T(8,128)(2,1)S(1)}, bf16[96,128]{1,0:T(8,128)(2,1)S(1)}, u32[]{:S(2)}, u32[]{:S(2)}) collective-permute-start(bf16[96,128]{1,0:T(8,128)(2,1)S(1)} %get-tuple-element.79), channel_id=1, source_target_pairs={{0,5},{1,4},{2,7},{3,6},{4,1},{5,0},{6,3},{7,2},{8,13},{9,12},{10,... | collective-permute-start | bytes 73736 | tf_op jit(solution)/shard_map/ppermute | solution.py:322
  43.3 5.2 %collective-permute-start.21 = (bf16[96,128]{1,0:T(8,128)(2,1)S(1)}, bf16[96,128]{1,0:T(8,128)(2,1)S(1)}, u32[]{:S(2)}, u32[]{:S(2)}) collective-permute-start(bf16[96,128]{1,0:T(8,128)(2,1)S(1)} %get-tuple-element.80), channel_id=1, source_target_pairs={{0,7},{1,6},{2,5},{3,4},{4,3},{5,2},{6,1},{7,0},{8,15},{9,14},{10,... | collective-permute-start | bytes 73736 | tf_op jit(solution)/shard_map/ppermute | solution.py:322
  44.4 6.3 %collective-permute-start.10 = (bf16[16,2048]{1,0:T(8,128)(2,1)S(1)}, bf16[16,2048]{1,0:T(8,128)(2,1)S(1)}, u32[]{:S(2)}, u32[]{:S(2)}) collective-permute-start(bf16[16,2048]{1,0:T(8,128)(2,1)S(1)} %get-tuple-element.62), channel_id=1, source_target_pairs={{0,7},{1,6},{2,5},{3,4},{4,3},{5,2},{6,1},{7,0},{8,15},{9,14},{10,... | collective-permute-start | bytes 196616 | tf_op jit(solution)/shard_map/ppermute | solution.py:322
  47.0 4.8 %collective-permute-start.8 = (bf16[16,2048]{1,0:T(8,128)(2,1)S(1)}, bf16[16,2048]{1,0:T(8,128)(2,1)S(1)}, u32[]{:S(2)}, u32[]{:S(2)}) collective-permute-start(bf16[16,2048]{1,0:T(8,128)(2,1)S(1)} %get-tuple-element.60), channel_id=1, source_target_pairs={{0,3},{1,2},{2,1},{3,0},{4,7},{5,6},{6,5},{7,4},{8,11},{9,10},{10,... | collective-permute-start | bytes 196616 | tf_op jit(solution)/shard_map/ppermute | solution.py:322
  48.4 5.5 %collective-permute-start.9 = (bf16[16,2048]{1,0:T(8,128)(2,1)S(1)}, bf16[16,2048]{1,0:T(8,128)(2,1)S(1)}, u32[]{:S(2)}, u32[]{:S(2)}) collective-permute-start(bf16[16,2048]{1,0:T(8,128)(2,1)S(1)} %get-tuple-element.61), channel_id=1, source_target_pairs={{0,5},{1,4},{2,7},{3,6},{4,1},{5,0},{6,3},{7,2},{8,13},{9,12},{10,... | collective-permute-start | bytes 196616 | tf_op jit(solution)/shard_map/ppermute | solution.py:322
  49.1 4.8 %copy-start.4 = (f32[2048]{0:T(1024)S(1)}, f32[2048]{0:T(1024)}, u32[]{:S(2)}) copy-start(f32[2048]{0:T(1024)} %param.12) | copy-start | bytes 24580
